TPU v7x, 512 devices: a whole 4x4x16 slice. The times are simulated.
512 devices in a mesh: ep: 32 (over z, core), tp: 16 (over y, x).
Axes of the slice: x: 4, y: 4, z: 16, core: 2. Of those that a mesh axis runs over, the one named last changes fastest.
Arguments:
- tokens: bfloat16 [1024, 2048], P('ep'), may hold values from -6 to 6
- recurrent_head_state: float32 [1024, 16, 4096], P('ep', 'tp'), may hold values from -4 to 4
- first_norm_gain: float32 [2048], replicated, may hold values from 0.1 to 1.9
- receptance_matrix: bfloat16 [2048, 1024], P(None, 'tp'), may hold values from -0.125 to 0.125
- key_matrix: bfloat16 [2048, 1024], P(None, 'tp'), may hold values from -0.125 to 0.125
- value_matrix: bfloat16 [2048, 1024], P(None, 'tp'), may hold values from -0.125 to 0.125
- decay_matrix: bfloat16 [2048, 1024], P(None, 'tp'), may hold values from -0.125 to 0.125
- decay_offset: float32 [1024], P('tp'), may hold values from -3 to 0.5
- correction_offset: float32 [1024], P('tp'), may hold values from -2 to 2
- correction_key_factor: float32 [1024], P('tp'), may hold values from -1 to 1
- own_term_weight: float32 [1024], P('tp'), may hold values from -0.9 to 0.9
- head_norm_gain: float32 [1024], P('tp'), may hold values from 0.1 to 1.9
- output_matrix: bfloat16 [1024, 2048], P('tp'), may hold values from -0.1875 to 0.1875
- second_norm_gain: float32 [2048], replicated, may hold values from 0.1 to 1.9
- routing: int32 [1024, 2], replicated, may hold values from 0 to 31, all different within a row; in each aligned block of 32 rows (0 to 31, 32 to 63, ...) at most 4 rows name the same one
- routing_weight: float32 [1024, 2], P('ep'), may hold values from 0.1 to 1
- expert_gate_weight: bfloat16 [32, 2048, 4096], P('ep', None, 'tp'), may hold values from -0.125 to 0.125
- expert_up_weight: bfloat16 [32, 2048, 4096], P('ep', None, 'tp'), may hold values from -0.125 to 0.125
- expert_down_weight: bfloat16 [32, 4096, 2048], P('ep', 'tp'), may hold values from -0.125 to 0.125
- dense_gate_weight: bfloat16 [2048, 2816], P(None, 'ep'), may hold values from -0.125 to 0.125
- dense_up_weight: bfloat16 [2048, 2816], P(None, 'ep'), may hold values from -0.125 to 0.125
- dense_down_weight: bfloat16 [2816, 2048], P('ep'), may hold values from -0.109375 to 0.109375
- dense_gate_offset: float32 [2048], replicated, may hold values from -3 to 3
Outputs:
- layer_out: bfloat16 [1024, 2048], P(('ep', 'tp'))
- next_state: float32 [1024, 16, 4096], P('ep', 'tp')
Inputs may be any that keep to these rules, and one draw needn't show every extreme that they name: `routing`: each row names 2 different experts. In each aligned block of 32 rows no expert is named more than 4 times, a bound that some block reaches.
All inputs are finite; a program needn't handle non-finite values.
Results may differ from a plain program's by a relative error of at most 0.017.
Values may be sent and summed in bfloat16 or wider, within the bound.
A program may use at most 64 MiB of HBM per device.

v0:
```python
import jax
import jax.numpy as jnp
from jax import lax
from jax.sharding import PartitionSpec as P

HEAD_WIDTH = 64


def sent_to_all(shard, axis):
    devices = lax.axis_size(axis)
    return lax.all_to_all(
        jnp.broadcast_to(shard[None], (devices, *shard.shape)), axis, 0, 0, tiled=True
    )


def taken_together(shard, axis):
    return sent_to_all(shard, axis).astype(jnp.float32).sum(axis=0)


def in_one_piece(arrays, axis, split_dim, concat_dim, along):
    both = jnp.concatenate(arrays, axis=along)
    result, at, finished = (
        lax.all_to_all(both, axis, split_axis=split_dim, concat_axis=concat_dim, tiled=True),
        0,
        [],
    )
    for a in arrays:
        finished.append(lax.slice_in_dim(result, at, at + a.shape[along], axis=along))
        at += a.shape[along]
    return tuple(finished)


def cut_along(shard, dim, devices):
    dims = shard.shape
    tiles = shard.reshape(*dims[:dim], devices, dims[dim] // devices, *dims[dim + 1 :])
    return jnp.moveaxis(tiles, dim, 0)


def summed_on_arrival(shard, axis, dim):
    devices = lax.axis_size(axis)
    tiles = lax.all_to_all(cut_along(shard, dim, devices), axis, 0, 0, tiled=True)
    return jnp.sum(tiles.astype(jnp.float32), axis=0)


def sent_together(arrays, axis, split_dim, concat_dim, along):
    columns = [a.reshape(*a.shape[:along], -1) for a in arrays]
    both = jnp.concatenate(columns, axis=along)
    result, at, finished = (
        lax.all_to_all(both, axis, split_axis=split_dim, concat_axis=concat_dim, tiled=True),
        0,
        [],
    )
    for a, column in zip(arrays, columns):
        share = result[..., at : at + column.shape[along]]
        finished.append(share.reshape(*share.shape[:along], *a.shape[along:]))
        at += column.shape[along]
    return tuple(finished)


def rms_scale(rows, gain):
    floats = rows.astype(jnp.float32)
    return floats * lax.rsqrt(jnp.mean(floats * floats, axis=-1, keepdims=True) + 1e-06) * gain


def route_table(block_routes, experts, capacity):
    flat_routes = block_routes.reshape(-1)
    chosen = (flat_routes[:, None] == jnp.arange(experts, dtype=jnp.int32)[None, :]).astype(
        jnp.int32
    )
    before = jnp.cumsum(chosen, axis=0, dtype=jnp.int32) - chosen
    slot_index = jnp.sum(before * chosen, axis=1)
    slot_match = (slot_index[:, None] == jnp.arange(capacity, dtype=jnp.int32)[None, :]).astype(
        jnp.float32
    )
    dispatch_table = chosen.astype(jnp.float32)[:, :, None] * slot_match[:, None, :]
    return dispatch_table.reshape(block_routes.shape[0], block_routes.shape[1], experts, capacity)


def state_update(
    receptance_rows,
    key_matrix_rows,
    value_matrix_rows,
    decay_logits,
    recurrent_head_state,
    decay_offset,
    correction_offset,
    correction_key_factor,
    own_term_weight,
    head_norm_gain,
    head_width,
):
    seq_count = key_matrix_rows.shape[0]
    decay_factor = jnp.exp(-jnp.exp(decay_offset + decay_logits))
    in_rate = jax.nn.sigmoid(correction_offset + correction_key_factor * key_matrix_rows)
    key_in = key_matrix_rows * in_rate

    def split_heads(block):
        return block.reshape(seq_count, -1, head_width)

    keys_head = split_heads(key_matrix_rows)
    unit_keys = (
        keys_head
        * lax.rsqrt(jnp.mean(keys_head * keys_head, axis=-1, keepdims=True) + 1e-06)
        * head_width ** (-0.5)
    )
    rate_head = split_heads(in_rate)
    head_keys = split_heads(key_in)
    decay_head = split_heads(decay_factor)
    head_values = split_heads(value_matrix_rows)
    head_receptance = split_heads(receptance_rows)
    matrix = recurrent_head_state.reshape(seq_count, -1, head_width, head_width)
    removed = jnp.einsum("bhvk,bhk->bhv", matrix, unit_keys)
    updated = (
        matrix * decay_head[:, :, None, :]
        - removed[..., None] * (unit_keys * rate_head)[:, :, None, :]
        + head_values[..., None] * head_keys[:, :, None, :]
    )
    readout = jnp.einsum("bhvk,bhk->bhv", updated, head_receptance)
    center = jnp.mean(readout, axis=-1, keepdims=True)
    spread = jnp.mean(jnp.square(readout - center), axis=-1, keepdims=True)
    normalized_rows = (
        (readout - center) * lax.rsqrt(spread + 0.00064) * head_norm_gain.reshape(-1, head_width)
    )
    own_term_total = jnp.sum(
        head_receptance * head_keys * own_term_weight.reshape(-1, head_width),
        axis=-1,
        keepdims=True,
    )
    normalized_rows = normalized_rows + own_term_total * head_values
    return (
        normalized_rows.reshape(seq_count, -1).astype(jnp.bfloat16),
        updated.reshape(seq_count, -1, head_width * head_width),
    )


def local(
    tokens,
    recurrent_head_state,
    first_norm_gain,
    receptance_matrix,
    key_matrix,
    value_matrix,
    decay_matrix,
    decay_offset,
    correction_offset,
    correction_key_factor,
    own_term_weight,
    head_norm_gain,
    output_matrix,
    second_norm_gain,
    routing,
    routing_weight,
    expert_gate_weight,
    expert_up_weight,
    expert_down_weight,
    dense_gate_weight,
    dense_up_weight,
    dense_down_weight,
    dense_gate_offset,
):
    seq_count = tokens.shape[0]
    width = tokens.shape[1]
    group_index = lax.axis_index("ep")
    lane_index = lax.axis_index("tp")
    group_count = lax.axis_size("ep")
    lane_count = lax.axis_size("tp")
    normalized_rows = rms_scale(tokens, first_norm_gain).astype(jnp.bfloat16)
    receptance_rows = jnp.dot(
        normalized_rows, receptance_matrix, preferred_element_type=jnp.float32
    )
    key_matrix_rows = jnp.dot(normalized_rows, key_matrix, preferred_element_type=jnp.float32)
    value_matrix_rows = jnp.dot(normalized_rows, value_matrix, preferred_element_type=jnp.float32)
    decay_logits = jnp.dot(normalized_rows, decay_matrix, preferred_element_type=jnp.float32)
    head_outputs, next_state = state_update(
        receptance_rows,
        key_matrix_rows,
        value_matrix_rows,
        decay_logits,
        recurrent_head_state,
        decay_offset,
        correction_offset,
        correction_key_factor,
        own_term_weight,
        head_norm_gain,
        HEAD_WIDTH,
    )
    partial_out = jnp.dot(head_outputs, output_matrix, preferred_element_type=jnp.float32)
    hidden_sum = tokens.astype(jnp.float32) + taken_together(
        partial_out.astype(jnp.bfloat16), "tp"
    ).astype(jnp.float32)
    ffn_in = rms_scale(hidden_sum, second_norm_gain).astype(jnp.bfloat16)
    local_experts = expert_gate_weight.shape[0]
    top_count = routing.shape[1]
    expert_count = local_experts * group_count
    capacity = 2 * seq_count * top_count // expert_count
    per_lane = seq_count // lane_count
    own_routes = lax.dynamic_slice_in_dim(routing, group_index * seq_count, seq_count, 0)
    own_table = route_table(own_routes, expert_count, capacity)
    send_rows = jnp.einsum(
        "bkec,bd->ecd", own_table.astype(jnp.bfloat16), ffn_in, preferred_element_type=jnp.float32
    ).astype(jnp.bfloat16)
    lane_rows = lax.dynamic_slice_in_dim(ffn_in, lane_index * per_lane, per_lane, 0)
    dense_send = jnp.broadcast_to(lane_rows[None], (group_count, per_lane, width))
    expert_in, dense_in = in_one_piece((send_rows, dense_send), "ep", 0, 0, 1)
    rows_in = expert_in.reshape(group_count, local_experts, capacity, width).transpose(1, 0, 2, 3)
    rows_in = rows_in.reshape(local_experts, group_count * capacity, width)
    gate_pre = jnp.einsum(
        "lrd,ldf->lrf", rows_in, expert_gate_weight, preferred_element_type=jnp.float32
    )
    up_pre = jnp.einsum(
        "lrd,ldf->lrf", rows_in, expert_up_weight, preferred_element_type=jnp.float32
    )
    expert_hidden = (jax.nn.silu(gate_pre) * up_pre).astype(jnp.bfloat16)
    expert_part = jnp.einsum(
        "lrf,lfd->lrd", expert_hidden, expert_down_weight, preferred_element_type=jnp.float32
    )
    expert_out = summed_on_arrival(expert_part.astype(jnp.bfloat16), "tp", 2).astype(jnp.bfloat16)
    back_send = expert_out.reshape(local_experts, group_count, capacity, -1).transpose(1, 0, 2, 3)
    back_send = back_send.reshape(group_count * local_experts, capacity, -1)
    dense_rows = dense_in.reshape(group_count * per_lane, width)
    dense_hidden = (
        jax.nn.silu(jnp.dot(dense_rows, dense_gate_weight, preferred_element_type=jnp.float32))
        * jnp.dot(dense_rows, dense_up_weight, preferred_element_type=jnp.float32)
    ).astype(jnp.bfloat16)
    dense_part = jnp.dot(
        dense_hidden, dense_down_weight, preferred_element_type=jnp.float32
    ).astype(jnp.bfloat16)
    dense_part = dense_part.reshape(group_count, per_lane, width)
    back_experts, back_dense = sent_together((back_send, dense_part), "ep", 0, 0, 1)
    dense_sum = jnp.sum(back_dense.astype(jnp.float32), axis=0)
    weighted = jnp.einsum("bkec,bk->ecb", own_table, routing_weight)
    moe_slice = jnp.einsum("ecb,ecd->bd", weighted, back_experts.astype(jnp.float32))
    moe_rows = lax.all_to_all(moe_slice, "tp", split_axis=0, concat_axis=1, tiled=True)
    residual_rows = lax.dynamic_slice_in_dim(hidden_sum, lane_index * per_lane, per_lane, 0)
    layer_out = (residual_rows + moe_rows + jax.nn.sigmoid(dense_gate_offset) * dense_sum).astype(
        jnp.bfloat16
    )
    return (layer_out, next_state)


def solution(mesh):
    return jax.shard_map(
        local,
        mesh=mesh,
        in_specs=(
            P("ep", None),
            P("ep", "tp", None),
            P(),
            P(None, "tp"),
            P(None, "tp"),
            P(None, "tp"),
            P(None, "tp"),
            P("tp"),
            P("tp"),
            P("tp"),
            P("tp"),
            P("tp"),
            P("tp", None),
            P(),
            P(),
            P("ep", None),
            P("ep", None, "tp"),
            P("ep", None, "tp"),
            P("ep", "tp", None),
            P(None, "ep"),
            P(None, "ep"),
            P("ep", None),
            P(),
        ),
        out_specs=(P(("ep", "tp"), None), P("ep", "tp", None)),
        check_vma=False,
    )
```

profile of v0, /device:TPU:1, one launch (start us, length us, event | category | flops | bytes accessed | tf_op | source)
XLA Modules:
  0.0 193.7 jit_solution(10774298676175109607)
XLA Ops:
  0.7 1.1 fusion.16
  1.9 1.4 multiply_reduce_fusion.3
  3.3 2.3 %reduce.11 = f32[32,4096]{1,0:T(8,128)S(1)} reduce(f32[32,1,4096]{2,1,0:T(1,128)} %param.24, f32[]{:T(128)} %constant.55), dimensions={1}, to_apply=%param.24.reduce_sub_computation | reduce | bytes 1048580 | tf_op args[1]
  5.6 0.4 reshape.273
  6.1 0.3 fusion.50
  6.4 1.3 multiply_reduce_fusion.1
  7.7 0.4 fusion.56
  8.1 1.3 fusion.5
  9.3 0.9 fusion.11
  10.6 0.2 convolution_convert_fusion.3
  10.8 1.6 broadcast_in_dim.4
  12.4 7.6 %all-to-all-start = ((bf16[16,32,2048]{2,1,0:T(8,128)(2,1)}), bf16[16,32,2048]{2,1,0:T(8,128)(2,1)S(1)}, u32[]{:S(2)}, u32[]{:S(2)}) async-start(bf16[16,32,2048]{2,1,0:T(8,128)(2,1)} %broadcast_in_dim.4), calls=%async_computation | async-start | bytes 4194304 | tf_op jit(solution)/shard_map/all_to_all | solution.py:11
  20.0 0.8 constant_dynamic-slice_fusion.1
  21.7 23.6 %all-to-all-done = bf16[16,32,2048]{2,1,0:T(8,128)(2,1)S(1)} async-done(((bf16[16,32,2048]{2,1,0:T(8,128)(2,1)}), bf16[16,32,2048]{2,1,0:T(8,128)(2,1)S(1)}, u32[]{:S(2)}, u32[]{:S(2)}) %all-to-all-start) | async-done | bytes 2097184 | tf_op jit(solution)/shard_map/all_to_all | solution.py:11
  45.3 0.4 convert_reduce_fusion
  46.0 0.3 convolution_convert_fusion.1
  46.3 0.2 copy-done.3
  46.7 1.5 copy.51
  48.1 22.8 %all-to-all-start.1 = ((bf16[32,6,2048]{2,1,0:T(8,128)(2,1)}), bf16[32,6,2048]{2,1,0:T(8,128)(2,1)}, u32[]{:S(2)}, u32[]{:S(2)}) async-start(bf16[32,6,2048]{2,1,0:T(8,128)(2,1)} %copy.51), calls=%async_computation.1 | async-start | bytes 2097152 | tf_op jit(solution)/shard_map/all_to_all | solution.py:23
  71.1 0.2 fusion.25
  71.3 0.6 copy.63
  71.9 0.6 broadcast_multiply_fusion
  72.6 1.5 mul.280
  74.0 0.7 mul.279
  74.7 0.7 mul.277
  75.4 51.2 %all-to-all-done.1 = bf16[32,6,2048]{2,1,0:T(8,128)(2,1)} async-done(((bf16[32,6,2048]{2,1,0:T(8,128)(2,1)}), bf16[32,6,2048]{2,1,0:T(8,128)(2,1)}, u32[]{:S(2)}, u32[]{:S(2)}) %all-to-all-start.1) | async-done | bytes 786464 | tf_op jit(solution)/shard_map/all_to_all | solution.py:23
  126.6 1.4 slice.16
  128.2 1.5 fusion.9
  129.8 2.0 %fusion = bf16[16,8,16,128]{3,1,2,0:T(8,128)(2,1)S(1)} fusion(bf16[1,256,2048]{2,1,0:T(8,128)(2,1)S(1)} %copy-done, bf16[128,2048]{1,0:T(8,128)(2,1)S(1)} %reshape.274, bf16[1,2048,256]{2,1,0:T(8,128)(2,1)} %param.40, f32[128,256]{1,0:T(8,128)S(1)} %fusion.9), kind=kOutput, calls=%fused_computation.5 | convolution fusion | flops 268894208 | bytes 3276800 | tf_op jit(solution)/shard_map/lrf,lfd->lrd/dot_general | solution.py:214
  131.9 0.9 copy.79
  132.8 4.2 %all-to-all-start.2 = ((bf16[16,1,128,128]{3,2,1,0:T(8,128)(2,1)}), bf16[16,1,128,128]{3,2,1,0:T(8,128)(2,1)}, u32[]{:S(2)}, u32[]{:S(2)}) async-start(bf16[16,1,128,128]{3,2,1,0:T(8,128)(2,1)} %bitcast.77), calls=%async_computation.2 | async-start | bytes 1048576 | tf_op jit(solution)/shard_map/all_to_all | solution.py:41
  137.1 1.5 slice.17
  138.7 0.2 fusion.57
  139.0 1.7 convolution_convert_fusion.2
  140.8 7.1 %all-to-all-done.2 = bf16[16,1,128,128]{3,2,1,0:T(8,128)(2,1)} async-done(((bf16[16,1,128,128]{3,2,1,0:T(8,128)(2,1)}), bf16[16,1,128,128]{3,2,1,0:T(8,128)(2,1)}, u32[]{:S(2)}, u32[]{:S(2)}) %all-to-all-start.2) | async-done | bytes 524320 | tf_op jit(solution)/shard_map/all_to_all | solution.py:41
  147.9 1.1 reduce_sum.113
  149.1 0.5 broadcast.176
  149.6 1.5 reduce.12
  151.1 1.7 reshape.291
  152.9 5.2 %all-to-all-start.3 = ((bf16[32,2,2304]{2,1,0:T(2,128)(2,1)}), bf16[32,2,2304]{2,1,0:T(2,128)(2,1)S(1)}, u32[]{:S(2)}, u32[]{:S(2)}) async-start(bf16[32,2,2304]{2,1,0:T(2,128)(2,1)} %reshape.291), calls=%async_computation.3 | async-start | bytes 589824 | tf_op jit(solution)/shard_map/all_to_all | solution.py:49
  158.1 1.9 %subtract_add_fusion = f32[4,8,4096]{2,1,0:T(8,128)} fusion(f32[4,8,4096]{2,1,0:T(8,128)S(1)} %bitcast.84, f32[4,8,4096]{2,1,0:T(8,128)S(1)} %bitcast.85, f32[4,8,4096]{2,1,0:T(8,128)} %bitcast.87, f32[4,8,4096]{2,1,0:T(8,128)S(1)} %bitcast.86), kind=kLoop, calls=%fused_computation.25 | loop fusion | flops 393216 | bytes 2621440 | tf_op jit(solution)/shard_map/add | solution.py:114
  160.0 21.2 %all-to-all-done.3 = bf16[32,2,2304]{2,1,0:T(2,128)(2,1)S(1)} async-done(((bf16[32,2,2304]{2,1,0:T(2,128)(2,1)}), bf16[32,2,2304]{2,1,0:T(2,128)(2,1)S(1)}, u32[]{:S(2)}, u32[]{:S(2)}) %all-to-all-start.3) | async-done | bytes 294944 | tf_op jit(solution)/shard_map/all_to_all | solution.py:49
  181.3 0.2 reshape.292
  181.6 0.2 convolution_bitcast_fusion
  181.8 0.6 copy.56
  182.4 3.5 %all-to-all-start.4 = ((f32[16,2,128]{2,1,0:T(2,128)}), f32[16,2,128]{2,1,0:T(2,128)S(1)}, u32[]{:S(2)}, u32[]{:S(2)}) async-start(f32[16,2,128]{2,1,0:T(2,128)} %copy.56), calls=%async_computation.4 | async-start | bytes 32768 | tf_op jit(solution)/shard_map/all_to_all | solution.py:233
  186.0 6.3 %all-to-all-done.4 = f32[16,2,128]{2,1,0:T(2,128)S(1)} async-done(((f32[16,2,128]{2,1,0:T(2,128)}), f32[16,2,128]{2,1,0:T(2,128)S(1)}, u32[]{:S(2)}, u32[]{:S(2)}) %all-to-all-start.4) | async-done | bytes 16416 | tf_op jit(solution)/shard_map/all_to_all | solution.py:233
  192.3 1.5 fusion.37
  (68 shorter events, 2.6 us)
Async XLA Ops:
  0.6 129.1 %copy-start = (bf16[1,256,2048]{2,1,0:T(8,128)(2,1)S(1)}, bf16[1,256,2048]{2,1,0:T(8,128)(2,1)}, u32[]{:S(2)}) copy-start(bf16[1,256,2048]{2,1,0:T(8,128)(2,1)} %param.41) | copy-start | bytes 3145732
  0.6 5.4 %copy-start.2 = (bf16[32,2048]{1,0:T(8,128)(2,1)S(1)}, bf16[32,2048]{1,0:T(8,128)(2,1)}, u32[]{:S(2)}) copy-start(bf16[32,2048]{1,0:T(8,128)(2,1)} %param.23) | copy-start | bytes 393220
  0.7 5.4 %copy-start.8 = (f32[2048]{0:T(1024)S(1)}, f32[2048]{0:T(1024)}, u32[]{:S(2)}) copy-start(f32[2048]{0:T(1024)} %param.25) | copy-start | bytes 24580
  0.7 5.4 %copy-start.5 = (bf16[2048,64]{0,1:T(8,128)(2,1)S(1)}, bf16[2048,64]{0,1:T(8,128)(2,1)}, u32[]{:S(2)}) copy-start(bf16[2048,64]{0,1:T(8,128)(2,1)} %param.28) | copy-start | bytes 786436
  0.7 5.7 %copy-start.15 = (f32[64]{0:T(128)S(1)}, f32[64]{0:T(128)}, u32[]{:S(2)}) copy-start(f32[64]{0:T(128)} %param.31) | copy-start | bytes 772
  0.7 5.7 %copy-start.14 = (f32[64]{0:T(128)S(1)}, f32[64]{0:T(128)}, u32[]{:S(2)}) copy-start(f32[64]{0:T(128)} %param.32) | copy-start | bytes 772
  0.7 5.7 %copy-start.13 = (f32[64]{0:T(128)S(1)}, f32[64]{0:T(128)}, u32[]{:S(2)}) copy-start(f32[64]{0:T(128)} %param.33) | copy-start | bytes 772
  3.3 4.8 %copy-start.16 = (f32[64]{0:T(128)S(1)}, f32[64]{0:T(128)}, u32[]{:S(2)}) copy-start(f32[64]{0:T(128)} %param.30) | copy-start | bytes 772
  6.0 4.5 %copy-start.6 = (bf16[64,2048]{1,0:T(8,128)(2,1)S(1)}, bf16[64,2048]{1,0:T(8,128)(2,1)}, u32[]{:S(2)}) copy-start(bf16[64,2048]{1,0:T(8,128)(2,1)} %param.35) | copy-start | bytes 786436
  6.1 4.5 %copy-start.12 = (f32[64]{0:T(128)S(1)}, f32[64]{0:T(128)}, u32[]{:S(2)}) copy-start(f32[64]{0:T(128)} %param.34) | copy-start | bytes 772
  12.4 32.9 %all-to-all-start = ((bf16[16,32,2048]{2,1,0:T(8,128)(2,1)}), bf16[16,32,2048]{2,1,0:T(8,128)(2,1)S(1)}, u32[]{:S(2)}, u32[]{:S(2)}) async-start(bf16[16,32,2048]{2,1,0:T(8,128)(2,1)} %broadcast_in_dim.4), calls=%async_computation | async-start | bytes 4194304 | tf_op jit(solution)/shard_map/all_to_all | solution.py:11
  20.0 25.8 %copy-start.9 = (f32[2048]{0:T(1024)S(1)}, f32[2048]{0:T(1024)}, u32[]{:S(2)}) copy-start(f32[2048]{0:T(1024)} %param.36) | copy-start | bytes 24580
  45.8 0.7 copy-start.3
  46.6 24.3 %copy-start.11 = (f32[32,2]{0,1:T(2,128)S(1)}, f32[32,2]{0,1:T(2,128)}, u32[]{:S(2)}) copy-start(f32[32,2]{0,1:T(2,128)} %param.38) | copy-start | bytes 772
  48.1 78.5 %all-to-all-start.1 = ((bf16[32,6,2048]{2,1,0:T(8,128)(2,1)}), bf16[32,6,2048]{2,1,0:T(8,128)(2,1)}, u32[]{:S(2)}, u32[]{:S(2)}) async-start(bf16[32,6,2048]{2,1,0:T(8,128)(2,1)} %copy.51), calls=%async_computation.1 | async-start | bytes 2097152 | tf_op jit(solution)/shard_map/all_to_all | solution.py:23
  131.8 6.9 %copy-start.4 = (bf16[2048,88]{0,1:T(8,128)(2,1)S(1)}, bf16[2048,88]{0,1:T(8,128)(2,1)}, u32[]{:S(2)}) copy-start(bf16[2048,88]{0,1:T(8,128)(2,1)} %param.42) | copy-start | bytes 1081348
  132.8 15.1 %all-to-all-start.2 = ((bf16[16,1,128,128]{3,2,1,0:T(8,128)(2,1)}), bf16[16,1,128,128]{3,2,1,0:T(8,128)(2,1)}, u32[]{:S(2)}, u32[]{:S(2)}) async-start(bf16[16,1,128,128]{3,2,1,0:T(8,128)(2,1)} %bitcast.77), calls=%async_computation.2 | async-start | bytes 1048576 | tf_op jit(solution)/shard_map/all_to_all | solution.py:41
  139.0 19.1 %copy-start.10 = (f32[2048]{0:T(1024)S(1)}, f32[2048]{0:T(1024)}, u32[]{:S(2)}) copy-start(f32[2048]{0:T(1024)} %param.45) | copy-start | bytes 24580
  139.0 19.1 %copy-start.1 = (f32[32,1,4096]{2,1,0:T(1,128)S(1)}, f32[32,1,4096]{2,1,0:T(1,128)}, u32[]{:S(2)}) copy-start(f32[32,1,4096]{2,1,0:T(1,128)} %mul.280) | copy-start | bytes 1572868
  152.9 28.4 %all-to-all-start.3 = ((bf16[32,2,2304]{2,1,0:T(2,128)(2,1)}), bf16[32,2,2304]{2,1,0:T(2,128)(2,1)S(1)}, u32[]{:S(2)}, u32[]{:S(2)}) async-start(bf16[32,2,2304]{2,1,0:T(2,128)(2,1)} %reshape.291), calls=%async_computation.3 | async-start | bytes 589824 | tf_op jit(solution)/shard_map/all_to_all | solution.py:49
  158.1 23.5 %copy-start.7 = (bf16[32,1,32,4]{2,0,3,1:T(8,128)(2,1)S(1)}, bf16[32,1,32,4]{2,0,3,1:T(8,128)(2,1)}, u32[]{:S(2)}) copy-start(bf16[32,1,32,4]{2,0,3,1:T(8,128)(2,1)} %copy.63) | copy-start | bytes 24580
  182.4 9.9 %all-to-all-start.4 = ((f32[16,2,128]{2,1,0:T(2,128)}), f32[16,2,128]{2,1,0:T(2,128)S(1)}, u32[]{:S(2)}, u32[]{:S(2)}) async-start(f32[16,2,128]{2,1,0:T(2,128)} %copy.56), calls=%async_computation.4 | async-start | bytes 32768 | tf_op jit(solution)/shard_map/all_to_all | solution.py:233
where the time goes:
time: 195 us; the launch traced here: 194 us
  waiting for transfers between devices  109 us (56%)
  starting transfers between devices  43.2 us (22%)
  local copies, waits for them, and re-layouts  16 us (8%)
  matrix products  11.9 us (6%)
  other arithmetic  11.8 us (6%)
    all_to_all x1, waiting for transfers between devices, in_one_piece(): lax.all_to_all(both, axis, split_axis=split_dim, concat_axis=concat_dim,...  51.2 us
    all_to_all x1, waiting for transfers between devices, sent_to_all(): lax.all_to_all(jnp.broadcast_to(shard[None], (devices, *shard.shape)), ax...  23.6 us
    all_to_all x1, starting transfers between devices, in_one_piece(): lax.all_to_all(both, axis, split_axis=split_dim, concat_axis=concat_dim,...  22.8 us
    all_to_all x1, waiting for transfers between devices, sent_together(): lax.all_to_all(both, axis, split_axis=split_dim, concat_axis=concat_dim,...  21.2 us
    all_to_all x1, starting transfers between devices, sent_to_all(): lax.all_to_all(jnp.broadcast_to(shard[None], (devices, *shard.shape)), ax...  7.57 us
    all_to_all x1, waiting for transfers between devices, summed_on_arrival(): lax.all_to_all(cut_along(shard, dim, devices), axis, 0, 0, tiled=True)  7.13 us
    all_to_all x1, waiting for transfers between devices, local(): lax.all_to_all(moe_slice, 'tp', split_axis=0, concat_axis=1, tiled=True)  6.29 us
    all_to_all x1, starting transfers between devices, sent_together(): lax.all_to_all(both, axis, split_axis=split_dim, concat_axis=concat_dim,...  5.18 us
  transfers between devices with their start and end apart: 5, of which 5 were waited for; matrix products, arithmetic and copies ran while one was open for 6% of the time, Pallas kernels for 0%

commit v1 on v0

v1 whole, which is shorter than its diff:
```python
import functools

import jax
import jax.numpy as jnp
from jax import lax
from jax.experimental import pallas as pl
from jax.experimental.pallas import tpu as pltpu
from jax.sharding import PartitionSpec as P

HEAD_WIDTH = 64
MESH = pl.DeviceIdType.MESH
F32 = jnp.float32
BF16 = jnp.bfloat16


def sigmoid(x):
    return 1.0 / (1.0 + jnp.exp(-x))


def layer_kernel(sizes, *refs):
    groups, lanes, seqs, width, experts, cap = sizes
    per_lane = seqs // lanes
    part = width // lanes
    pair = 2 * HEAD_WIDTH
    tiles = HEAD_WIDTH // 2
    (
        tokens_hbm, state_hbm, gain1_hbm, wr_hbm, wk_hbm, wv_hbm, wd_hbm,
        doff_hbm, coff_hbm, ckey_hbm, own_hbm, hgain_hbm, wout_hbm, gain2_hbm,
        routes_hbm, rweight_hbm, eg_hbm, eu_hbm, ed_hbm, dg_hbm, du_hbm, dd_hbm, goff_hbm,
        out_ref, next_hbm,
        tok, state, gain1, joined, doff, coff, ckey, own, hgain, wout, gain2,
        routes, rweight, eg, eu, ed, dense_up, dd, goff,
        next_state, tokf, wide, slots,
        col_send, row_send, col_in, row_in, hidden,
        disp_send, disp_in, rows_all, dense_send, dense_in, dense_rows, dback_send, dback_in,
        eo_send, eo_in, back_send, back_in, moe_send, moe_in, moe_wide,
        load_sem, store_sem, send_sem, recv_sem,
    ) = refs
    g = lax.axis_index("ep")
    t = lax.axis_index("tp")
    my_part = pl.ds(pl.multiple_of(t * part, part), part)

    wr, wk, wv, wd = (joined.at[pl.ds(i * HEAD_WIDTH, HEAD_WIDTH)] for i in range(4))
    units = dg_hbm.shape[0]
    dg, du = (dense_up.at[pl.ds(i * 128, units)] for i in range(2))
    sources = (
        tokens_hbm, gain1_hbm, wr_hbm, wk_hbm, wv_hbm, wd_hbm, doff_hbm, coff_hbm, ckey_hbm, own_hbm, hgain_hbm,
        state_hbm, wout_hbm, routes_hbm, rweight_hbm, gain2_hbm, eg_hbm, eu_hbm, dg_hbm, du_hbm, ed_hbm, dd_hbm, goff_hbm,
    )
    targets = (
        tok, gain1, wr, wk, wv, wd, doff, coff, ckey, own, hgain,
        state, wout, routes, rweight, gain2, eg, eu, dg, du, ed, dd, goff,
    )
    loads = {
        id(to): pltpu.make_async_copy(frm, to, load_sem.at[i])
        for i, (frm, to) in enumerate(zip(sources, targets))
    }
    for to in targets:
        loads[id(to)].start()

    def arrived(*buffers):
        for to in buffers:
            loads[id(to)].wait()

    barrier = pltpu.get_barrier_semaphore()

    @pl.loop(1, lanes)
    def _(p):
        pl.semaphore_signal(barrier, inc=1, device_id=(g, lax.rem(t + p, lanes)), device_id_type=MESH)

    @pl.loop(1, groups)
    def _(p):
        pl.semaphore_signal(barrier, inc=1, device_id=(lax.rem(g + p, groups), t), device_id_type=MESH)

    def over_lanes(stage, source, target):
        @pl.loop(1, lanes)
        def _(p):
            peer = lax.rem(t + p, lanes)
            pltpu.make_async_remote_copy(
                src_ref=source(peer), dst_ref=target, send_sem=send_sem.at[stage],
                recv_sem=recv_sem.at[stage], device_id=(g, peer), device_id_type=MESH,
            ).start()

    def over_groups(stage, source, target):
        @pl.loop(1, groups)
        def _(p):
            peer = lax.rem(g + p, groups)
            pltpu.make_async_remote_copy(
                src_ref=source(peer), dst_ref=target, send_sem=send_sem.at[stage],
                recv_sem=recv_sem.at[stage], device_id=(peer, t), device_id_type=MESH,
            ).start()

    def descriptor(stage, ref):
        return pltpu.make_async_remote_copy(
            src_ref=ref, dst_ref=ref, send_sem=send_sem.at[stage], recv_sem=recv_sem.at[stage],
            device_id=(g, lax.rem(t + 1, lanes)), device_id_type=MESH,
        )

    arrived(tok, gain1)
    floats = tok[...].astype(F32)
    tokf[...] = floats
    normed = (
        floats * lax.rsqrt(jnp.mean(floats * floats, axis=-1, keepdims=True) + 1e-06) * gain1[...]
    ).astype(BF16)
    arrived(wr, wk, wv, wd)
    projected = lax.dot_general(normed, joined[...], (((1,), (1,)), ((), ())), preferred_element_type=F32)
    recept = projected[:, 0:HEAD_WIDTH]
    keys = projected[:, HEAD_WIDTH : 2 * HEAD_WIDTH]
    values = projected[:, 2 * HEAD_WIDTH : 3 * HEAD_WIDTH]
    decay_pre = projected[:, 3 * HEAD_WIDTH : 4 * HEAD_WIDTH]

    arrived(doff, coff, ckey, own, hgain)
    decay = jnp.exp(-jnp.exp(doff[...] + decay_pre))
    rate = sigmoid(coff[...] + ckey[...] * keys)
    key_in = keys * rate
    unit = keys * lax.rsqrt(jnp.mean(keys * keys, axis=-1, keepdims=True) + 1e-06) * HEAD_WIDTH**-0.5

    def twice(x):
        return jnp.concatenate([x, x], axis=1)

    decay2, unit2, rate2, key2, recept2, values2 = map(
        twice, (decay, unit, unit * rate, key_in, recept, values)
    )
    lane_of = lax.broadcasted_iota(jnp.int32, (seqs, pair), 1)
    low = lane_of < HEAD_WIDTH

    def halves(x):
        first = jnp.sum(jnp.where(low, x, 0.0), axis=-1, keepdims=True)
        second = jnp.sum(jnp.where(low, 0.0, x), axis=-1, keepdims=True)
        return first, second

    def picked(x, lane):
        return jnp.sum(jnp.where(lane_of == lane, x, 0.0), axis=-1, keepdims=True)

    arrived(state)
    at_once = 4

    def some_tiles(step, readout):
        for inner in range(at_once):
            c = step * at_once + inner
            rows = pl.ds(c, seqs, stride=tiles)
            block = state[rows, :]
            removed = jnp.where(low, *halves(block * unit2))
            added = jnp.where(low, picked(values2, 2 * c), picked(values2, 2 * c + 1))
            block = block * decay2 - removed * rate2 + added * key2
            next_state[rows, :] = block
            first, second = halves(block * recept2)
            readout = jnp.where(lane_of == 2 * c, first, readout)
            readout = jnp.where(lane_of == 2 * c + 1, second, readout)
        return readout

    readout = lax.fori_loop(0, tiles // at_once, some_tiles, jnp.zeros((seqs, pair), F32))
    store = pltpu.make_async_copy(next_state, next_hbm, store_sem)
    store.start()
    readout = readout[:, 0:HEAD_WIDTH]
    center = jnp.mean(readout, axis=-1, keepdims=True)
    spread = jnp.mean(jnp.square(readout - center), axis=-1, keepdims=True)
    heads = (readout - center) * lax.rsqrt(spread + 0.00064) * hgain[...]
    heads = heads + jnp.sum(recept * key_in * own[...], axis=-1, keepdims=True) * values
    heads = heads.astype(BF16)

    arrived(wout)
    share = jnp.dot(heads, wout[...], preferred_element_type=F32)
    wide[0:seqs, :] = share
    col_send[...] = share.astype(BF16)
    col_in[pl.ds(t, 1)] = col_send[:, my_part][None]
    pl.semaphore_wait(barrier, lanes + groups - 2)
    over_lanes(
        0, lambda peer: col_send.at[:, pl.ds(pl.multiple_of(peer * part, part), part)], col_in.at[t]
    )
    for p in range(lanes):
        row_send[p] = wide[p * per_lane : (p + 1) * per_lane, :].astype(BF16)
    row_in[pl.ds(t, 1)] = row_send[pl.ds(t, 1)]
    over_lanes(1, lambda peer: row_send.at[peer], row_in.at[t])

    arrived(routes, rweight)
    chunk = pl.ds(pl.multiple_of(g // (128 // seqs) * 128, 128), 128)
    offset = lax.rem(g, 128 // seqs) * seqs
    pick = (
        lax.broadcasted_iota(jnp.int32, (128, seqs), 0)
        == lax.broadcasted_iota(jnp.int32, (128, seqs), 1) + offset
    ).astype(BF16)
    own_routes = jnp.dot(
        routes[:, chunk].astype(F32).astype(BF16), pick, preferred_element_type=F32
    ).astype(jnp.int32)
    slot = lax.broadcasted_iota(jnp.int32, (experts * cap, seqs), 0)
    expert_of, place_of = slot // cap, lax.rem(slot, cap)
    first, second = own_routes[0:1] == expert_of, own_routes[1:2] == expert_of
    either = jnp.where(first | second, 1.0, 0.0).astype(BF16)
    earlier = (
        lax.broadcasted_iota(jnp.int32, (seqs, seqs), 0)
        < lax.broadcasted_iota(jnp.int32, (seqs, seqs), 1)
    ).astype(BF16)
    here = jnp.dot(either, earlier, preferred_element_type=F32).astype(jnp.int32) == place_of
    table = jnp.where((first | second) & here, 1.0, 0.0).astype(BF16)
    weighted = jnp.where(first & here, rweight[0:1], 0.0) + jnp.where(second & here, rweight[1:2], 0.0)

    mine = (
        lax.broadcasted_iota(jnp.int32, (per_lane, seqs), 1)
        == lax.broadcasted_iota(jnp.int32, (per_lane, seqs), 0) + t * per_lane
    ).astype(BF16)
    hidden[...] = jnp.dot(mine, tok[...], preferred_element_type=F32)

    arrived(gain2)
    descriptor(0, col_in.at[pl.ds(0, lanes - 1)]).wait_recv()
    total = tokf[:, my_part]
    for p in range(lanes):
        total = total + col_in[p].astype(F32)
    gained = (total * gain2[:, my_part]).astype(BF16)
    slots[...] = jnp.dot(table, gained, preferred_element_type=F32)
    for e in range(experts):
        disp_send[e] = slots[e * cap : (e + 1) * cap, :].astype(BF16)
    disp_in[pl.ds(g, 1)] = disp_send[pl.ds(g, 1)]
    over_groups(2, lambda peer: disp_send.at[peer], disp_in.at[g])

    descriptor(1, row_in.at[pl.ds(0, lanes - 1)]).wait_recv()
    total = hidden[...]
    for p in range(lanes):
        total = total + row_in[p].astype(F32)
    hidden[...] = total
    dense_send[...] = (
        total * lax.rsqrt(jnp.mean(total * total, axis=-1, keepdims=True) + 1e-06) * gain2[...]
    ).astype(BF16)
    dense_in[pl.ds(g, 1)] = dense_send[...][None]
    over_groups(3, lambda peer: dense_send, dense_in.at[g])

    descriptor(2, disp_in.at[pl.ds(0, groups - 1)]).wait_recv()
    for e in range(groups):
        slots[e * cap : (e + 1) * cap, :] = disp_in[e].astype(F32)
    rows_all[:, my_part] = slots[...].astype(BF16)
    over_lanes(4, lambda peer: rows_all.at[:, my_part], rows_all.at[:, my_part])

    inverse = 1.0 / (gain2[...] * gain2[...])
    arrived(eg, eu, ed)
    descriptor(4, rows_all.at[:, pl.ds(0, width - part)]).wait_recv()
    squares = jnp.zeros((groups * cap, part), F32)
    for p in range(lanes):
        piece = rows_all[:, p * part : (p + 1) * part].astype(F32)
        squares = squares + piece * piece * inverse[:, p * part : (p + 1) * part]
    scale = lax.rsqrt(jnp.sum(squares, axis=-1, keepdims=True) / width + 1e-06)
    gate = jnp.dot(rows_all[...], eg[0], preferred_element_type=F32) * scale
    up = jnp.dot(rows_all[...], eu[0], preferred_element_type=F32) * scale
    inner = (gate * sigmoid(gate) * up).astype(BF16)
    block = 2 * part
    for p in range(width // block):
        eo_send[:, p * block : (p + 1) * block] = jnp.dot(
            inner, ed[0, :, p * block : (p + 1) * block], preferred_element_type=F32
        ).astype(BF16)
    eo_in[pl.ds(t, 1)] = eo_send[:, my_part][None]
    over_lanes(
        5, lambda peer: eo_send.at[:, pl.ds(pl.multiple_of(peer * part, part), part)], eo_in.at[t]
    )

    arrived(dg, du, dd, goff)
    descriptor(3, dense_in.at[pl.ds(0, groups - 1)]).wait_recv()
    for e in range(groups):
        wide[e * per_lane : (e + 1) * per_lane, :] = dense_in[e].astype(F32)
    dense_rows[...] = wide[...].astype(BF16)
    both = lax.dot_general(
        dense_rows[...], dense_up[...], (((1,), (1,)), ((), ())), preferred_element_type=F32
    )
    gate, up = both[:, 0:units], both[:, 128 : 128 + units]
    inner = (gate * sigmoid(gate) * up).astype(BF16)
    wide[...] = jnp.dot(inner, dd[...], preferred_element_type=F32)
    for e in range(groups):
        dback_send[e] = wide[e * per_lane : (e + 1) * per_lane, :].astype(BF16)
    dback_in[pl.ds(g, 1)] = dback_send[pl.ds(g, 1)]

    descriptor(5, eo_in.at[pl.ds(0, lanes - 1)]).wait_recv()
    total = jnp.zeros((groups * cap, part), F32)
    for p in range(lanes):
        total = total + eo_in[p].astype(F32)
    slots[...] = total
    for e in range(groups):
        back_send[e] = slots[e * cap : (e + 1) * cap, :].astype(BF16)
    back_in[pl.ds(g, 1)] = back_send[pl.ds(g, 1)]
    over_groups(6, lambda peer: back_send.at[peer], back_in.at[g])
    over_groups(7, lambda peer: dback_send.at[peer], dback_in.at[g])

    upper = weighted.astype(BF16)
    lower = (weighted - upper.astype(F32)).astype(BF16)
    descriptor(6, back_in.at[pl.ds(0, groups - 1)]).wait_recv()
    for e in range(experts):
        slots[e * cap : (e + 1) * cap, :] = back_in[e].astype(F32)
    back = slots[...].astype(BF16)
    across = (((0,), (0,)), ((), ()))
    moe = lax.dot_general(upper, back, across, preferred_element_type=F32)
    moe = moe + lax.dot_general(lower, back, across, preferred_element_type=F32)
    slots[0:seqs, :] = moe
    for p in range(lanes):
        moe_send[p] = slots[p * per_lane : (p + 1) * per_lane, :]
    moe_in[pl.ds(t, 1)] = moe_send[pl.ds(t, 1)]
    over_lanes(8, lambda peer: moe_send.at[peer], moe_in.at[t])

    descriptor(7, dback_in.at[pl.ds(0, groups - 1)]).wait_recv()
    total = jnp.zeros((per_lane, width), F32)
    for e in range(groups):
        total = total + dback_in[e].astype(F32)
    base = hidden[...] + sigmoid(goff[...]) * total
    descriptor(8, moe_in.at[pl.ds(0, lanes - 1)]).wait_recv()
    for p in range(lanes):
        moe_wide[:, p * part : (p + 1) * part] = moe_in[p]
    out_ref[...] = (base + moe_wide[...]).astype(BF16)

    store.wait()
    descriptor(0, col_in.at[pl.ds(0, lanes - 1)]).wait_send()
    descriptor(1, row_in.at[pl.ds(0, lanes - 1)]).wait_send()
    descriptor(2, disp_in.at[pl.ds(0, groups - 1)]).wait_send()
    descriptor(3, dense_in.at[pl.ds(0, groups - 1)]).wait_send()
    descriptor(4, rows_all.at[:, pl.ds(0, width - part)]).wait_send()
    descriptor(5, eo_in.at[pl.ds(0, lanes - 1)]).wait_send()
    descriptor(6, back_in.at[pl.ds(0, groups - 1)]).wait_send()
    descriptor(7, dback_in.at[pl.ds(0, groups - 1)]).wait_send()
    descriptor(8, moe_in.at[pl.ds(0, lanes - 1)]).wait_send()


def local(*args):
    (
        tokens, state, gain1, wr, wk, wv, wd, doff, coff, ckey, own, hgain, wout, gain2,
        routing, rweight, eg, eu, ed, dg, du, dd, goff,
    ) = args
    groups, lanes = lax.axis_size("ep"), lax.axis_size("tp")
    seqs, width = tokens.shape
    top = routing.shape[1]
    experts = groups
    cap = 2 * seqs * top // experts
    per_lane, part = seqs // lanes, width // lanes
    rows = seqs * HEAD_WIDTH * HEAD_WIDTH // 128
    row = lambda v: v.reshape(1, -1)
    operands = (
        tokens, state.reshape(rows, 128), row(gain1), wr.T, wk.T, wv.T, wd.T, row(doff), row(coff), row(ckey), row(own),
        row(hgain), wout, row(gain2), routing.T, rweight.T, eg, eu, ed, dg.T, du.T, dd, row(goff),
    )
    vmem = pltpu.VMEM
    joined, dense_up = vmem((4 * HEAD_WIDTH, width), BF16), vmem((256, width), BF16)
    held = [vmem(a.shape, a.dtype) for a in operands]
    held = [*held[:3], joined, *held[7:19], dense_up, *held[21:]]
    sizes = (groups, lanes, seqs, width, experts, cap)
    scratch = held + [
        vmem((rows, 128), F32),
        vmem((seqs, width), F32),
        vmem((max(seqs, groups * per_lane), width), F32),
        vmem((groups * cap, part), F32),
        vmem((seqs, width), BF16),
        vmem((lanes, per_lane, width), BF16),
        vmem((lanes, seqs, part), BF16),
        vmem((lanes, per_lane, width), BF16),
        vmem((per_lane, width), F32),
        vmem((experts, cap, part), BF16),
        vmem((groups, cap, part), BF16),
        vmem((groups * cap, width), BF16),
        vmem((per_lane, width), BF16),
        vmem((groups, per_lane, width), BF16),
        vmem((groups * per_lane, width), BF16),
        vmem((groups, per_lane, width), BF16),
        vmem((groups, per_lane, width), BF16),
        vmem((groups * cap, width), BF16),
        vmem((lanes, groups * cap, part), BF16),
        vmem((groups, cap, part), BF16),
        vmem((experts, cap, part), BF16),
        vmem((lanes, per_lane, part), F32),
        vmem((lanes, per_lane, part), F32),
        vmem((per_lane, width), F32),
        pltpu.SemaphoreType.DMA((len(operands),)),
        pltpu.SemaphoreType.DMA,
        pltpu.SemaphoreType.DMA((9,)),
        pltpu.SemaphoreType.DMA((9,)),
    ]
    layer_out, next_state = pl.pallas_call(
        functools.partial(layer_kernel, sizes),
        out_shape=(
            jax.ShapeDtypeStruct((per_lane, width), BF16),
            jax.ShapeDtypeStruct((rows, 128), F32),
        ),
        in_specs=[pl.BlockSpec(memory_space=pl.ANY)] * len(operands),
        out_specs=(pl.BlockSpec(memory_space=pltpu.VMEM), pl.BlockSpec(memory_space=pl.ANY)),
        scratch_shapes=scratch,
        compiler_params=pltpu.CompilerParams(
            collective_id=0, has_side_effects=True, vmem_limit_bytes=60_000_000
        ),
        name="layer",
    )(*operands)
    return layer_out, next_state.reshape(state.shape)


def solution(mesh):
    return jax.shard_map(
        local,
        mesh=mesh,
        in_specs=(
            P("ep", None),
            P("ep", "tp", None),
            P(),
            P(None, "tp"),
            P(None, "tp"),
            P(None, "tp"),
            P(None, "tp"),
            P("tp"),
            P("tp"),
            P("tp"),
            P("tp"),
            P("tp"),
            P("tp", None),
            P(),
            P(),
            P("ep", None),
            P("ep", None, "tp"),
            P("ep", None, "tp"),
            P("ep", "tp", None),
            P(None, "ep"),
            P(None, "ep"),
            P("ep", None),
            P(),
        ),
        out_specs=(P(("ep", "tp"), None), P("ep", "tp", None)),
        check_vma=False,
    )
```

time: 195 us -> 73.7 us (0.38)
  waiting for transfers between devices: 109 us -> 0 us
  Pallas kernels: 0 us -> 69.7 us
  starting transfers between devices: 43.2 us -> 0 us
  local copies, waits for them, and re-layouts: 16 us -> 3.17 us
  matrix products: 11.9 us -> 0 us
  other arithmetic: 11.8 us -> 0 us
    all_to_all x5 -> x0, waiting for transfers between devices: 109 us -> none  [the longest x1 51.2 us: in_one_piece(): lax.all_to_all(both, axis, split_axis=split_dim, concat_axis=concat_dim,...]
    pallas_call x0 -> x1, Pallas kernels: none -> 69.7 us  [local(): pl.pallas_call(functools.partial(layer_kernel, sizes), out_shape=(jax.Sha...]
    all_to_all x5 -> x0, starting transfers between devices: 43.2 us -> none  [the longest x1 22.8 us: in_one_piece(): lax.all_to_all(both, axis, split_axis=split_dim, concat_axis=concat_dim,...]
    dot_general x14 -> x0, matrix products: 11.9 us -> none  [the longest x1 2 us: local(): jnp.einsum('lrf,lfd->lrd', expert_hidden, expert_down_weight, preferred_e...]
    reduce_sum x9 -> x0, other arithmetic: 3.44 us -> none  [the longest x2 1.29 us: rms_scale(): jnp.mean(floats * floats, axis=-1, keepdims=True) + 1e-06]
    slice x2 -> x0, local copies, waits for them, and re-layouts: 2.96 us -> none  [in_one_piece(): lax.slice_in_dim(result, at, at + a.shape[along], axis=along)]
    mul x4 -> x0, local copies, waits for them, and re-layouts: 2.82 us -> none  [the longest x1 1.45 us: state_update(): head_values[..., None] * head_keys[:, :, None, :]]
    unnamed x1 -> x0, other arithmetic: 2.3 us -> none
  transfers between devices with their start and end apart: 5 -> 0, of which waited for: 5 -> 0; matrix products, arithmetic and copies ran while one was open for 6% -> 0% of each run, Pallas kernels for 0% -> 0%
where the time goes in v1:
time: 73.7 us; the launch traced here: 73.5 us
  Pallas kernels  69.7 us (95%)
  local copies, waits for them, and re-layouts  3.17 us (4%)
    pallas_call x1, Pallas kernels, local(): pl.pallas_call(functools.partial(layer_kernel, sizes), out_shape=(jax.Sha...  69.7 us
    unnamed x2, local copies, waits for them, and re-layouts  3.17 us

profile of v1, /device:TPU:1, one launch (start us, length us, event | category | flops | bytes accessed | tf_op | source)
XLA Modules:
  0.0 73.5 jit_solution(3540615162104162103)
XLA Ops:
  0.6 69.7 %layer.1 = (bf16[2,2048]{1,0:T(2,128)(2,1)}, f32[1024,128]{1,0:T(8,128)}) custom-call(bf16[32,2048]{1,0:T(8,128)(2,1)} %refs_0_.1, f32[1024,128]{1,0:T(8,128)} %bitcast.18, f32[1,2048]{1,0:T(1,128)} %bitcast.26, bf16[64,2048]{1,0:T(8,128)(2,1)} %bitcast.22, bf16[64,2048]{1,0:T(8,128)(2,1)} %bitcast.23, bf16[64,2048]{1,0:T(8,128)(2,1)} %bitcast.24, ...), custom_call_target="tpu_custom_call" | custom-call | tf_op jit(solution)/shard_map/layer/pallas_call | solution.py:369
  70.3 1.3 %copy.28 = bf16[2,2048]{1,0:T(2,128)(2,1)} copy(bf16[2,2048]{1,0:T(2,128)(2,1)} %get-tuple-element.10) | data formatting | bytes 16384
  71.6 1.9 %copy.29 = f32[32,1,4096]{2,1,0:T(1,128)} copy(f32[32,1,4096]{2,1,0:T(1,128)} %bitcast.19) | data formatting | bytes 1048576

commit v2 on v1

--- a/solution.py
+++ b/solution.py
@@ -27,18 +27,31 @@
         tokens_hbm, state_hbm, gain1_hbm, wr_hbm, wk_hbm, wv_hbm, wd_hbm,
         doff_hbm, coff_hbm, ckey_hbm, own_hbm, hgain_hbm, wout_hbm, gain2_hbm,
         routes_hbm, rweight_hbm, eg_hbm, eu_hbm, ed_hbm, dg_hbm, du_hbm, dd_hbm, goff_hbm,
-        out_ref, next_hbm,
+        out_ref, next_state,
         tok, state, gain1, joined, doff, coff, ckey, own, hgain, wout, gain2,
         routes, rweight, eg, eu, ed, dense_up, dd, goff,
-        next_state, tokf, wide, slots,
+        wide, slots,
         col_send, row_send, col_in, row_in, hidden,
-        disp_send, disp_in, rows_all, dense_send, dense_in, dense_rows, dback_send, dback_in,
+        disp_send, disp_in, rows_all, dense_send, dense_in, dense_rows, dback_send, dback_in, pair_in, chip_sum,
         eo_send, eo_in, back_send, back_in, moe_send, moe_in, moe_wide,
-        load_sem, store_sem, send_sem, recv_sem,
+        load_sem, send_sem, recv_sem,
     ) = refs
     g = lax.axis_index("ep")
     t = lax.axis_index("tp")
+    chips, chip, core = groups // 2, g // 2, lax.rem(g, 2)
+    partner = g + 1 - 2 * core
+    quarter, half = chips // 4, groups * cap // 2
     my_part = pl.ds(pl.multiple_of(t * part, part), part)
+
+    barrier = pltpu.get_barrier_semaphore()
+
+    @pl.loop(1, lanes)
+    def _(p):
+        pl.semaphore_signal(barrier, inc=1, device_id=(g, lax.rem(t + p, lanes)), device_id_type=MESH)
+
+    @pl.loop(1, groups)
+    def _(p):
+        pl.semaphore_signal(barrier, inc=1, device_id=(lax.rem(g + p, groups), t), device_id_type=MESH)
 
     wr, wk, wv, wd = (joined.at[pl.ds(i * HEAD_WIDTH, HEAD_WIDTH)] for i in range(4))
     units = dg_hbm.shape[0]
@@ -61,16 +74,6 @@
     def arrived(*buffers):
         for to in buffers:
             loads[id(to)].wait()
-
-    barrier = pltpu.get_barrier_semaphore()
-
-    @pl.loop(1, lanes)
-    def _(p):
-        pl.semaphore_signal(barrier, inc=1, device_id=(g, lax.rem(t + p, lanes)), device_id_type=MESH)
-
-    @pl.loop(1, groups)
-    def _(p):
-        pl.semaphore_signal(barrier, inc=1, device_id=(lax.rem(g + p, groups), t), device_id_type=MESH)
 
     def over_lanes(stage, source, target):
         @pl.loop(1, lanes)
@@ -81,14 +84,56 @@
                 recv_sem=recv_sem.at[stage], device_id=(g, peer), device_id_type=MESH,
             ).start()
 
-    def over_groups(stage, source, target):
-        @pl.loop(1, groups)
-        def _(p):
-            peer = lax.rem(g + p, groups)
-            pltpu.make_async_remote_copy(
-                src_ref=source(peer), dst_ref=target, send_sem=send_sem.at[stage],
-                recv_sem=recv_sem.at[stage], device_id=(peer, t), device_id_type=MESH,
-            ).start()
+    def to_device(stage, source, target, peer):
+        pltpu.make_async_remote_copy(
+            src_ref=source, dst_ref=target, send_sem=send_sem.at[stage],
+            recv_sem=recv_sem.at[stage], device_id=(peer, t), device_id_type=MESH,
+        ).start()
+
+    def to_experts():
+        @pl.loop(chips // 2, chips)
+        def _(j):
+            for c in range(2):
+                peer = lax.rem(chip + quarter - j + chips, chips) * 2 + c
+                to_device(3, disp_send.at[peer], disp_in.at[2 * j + core], peer)
+
+        @pl.loop(1, chips // 2)
+        def _(k):
+            j = lax.rem(quarter + k, chips // 2)
+            for c in range(2):
+                peer = lax.rem(chip + quarter - j + chips, chips) * 2 + c
+                to_device(2, disp_send.at[peer], disp_in.at[2 * j + core], peer)
+
+        to_device(2, disp_send.at[partner], disp_in.at[2 * quarter + core], partner)
+
+    def to_groups_near():
+        @pl.loop(1, chips // 2)
+        def _(k):
+            j = lax.rem(quarter + k, chips // 2)
+            for c in range(2):
+                peer = lax.rem(chip + j - quarter + chips, chips) * 2 + c
+                to_device(8, back_send.at[2 * j + c], back_in.at[g], peer)
+
+        to_device(8, back_send.at[2 * quarter + 1 - core], back_in.at[g], partner)
+
+    def to_groups_far():
+        @pl.loop(chips // 2, chips)
+        def _(j):
+            for c in range(2):
+                peer = lax.rem(chip + j - quarter + chips, chips) * 2 + c
+                to_device(8, back_send.at[2 * j + c], back_in.at[g], peer)
+
+    def over_chips(stage, source, target):
+        def send(distance):
+            peer = lax.rem(chip + distance, chips)
+            to_device(stage, source(peer), target, 2 * peer + core)
+
+        send(chips // 2)
+
+        @pl.loop(1, chips // 2)
+        def _(k):
+            send(chips // 2 - k)
+            send(chips // 2 + k)
 
     def descriptor(stage, ref):
         return pltpu.make_async_remote_copy(
@@ -98,7 +143,6 @@
 
     arrived(tok, gain1)
     floats = tok[...].astype(F32)
-    tokf[...] = floats
     normed = (
         floats * lax.rsqrt(jnp.mean(floats * floats, axis=-1, keepdims=True) + 1e-06) * gain1[...]
     ).astype(BF16)
@@ -150,8 +194,6 @@
         return readout
 
     readout = lax.fori_loop(0, tiles // at_once, some_tiles, jnp.zeros((seqs, pair), F32))
-    store = pltpu.make_async_copy(next_state, next_hbm, store_sem)
-    store.start()
     readout = readout[:, 0:HEAD_WIDTH]
     center = jnp.mean(readout, axis=-1, keepdims=True)
     spread = jnp.mean(jnp.square(readout - center), axis=-1, keepdims=True)
@@ -160,18 +202,12 @@
     heads = heads.astype(BF16)
 
     arrived(wout)
-    share = jnp.dot(heads, wout[...], preferred_element_type=F32)
-    wide[0:seqs, :] = share
-    col_send[...] = share.astype(BF16)
+    col_send[...] = jnp.dot(heads, wout[...], preferred_element_type=F32).astype(BF16)
     col_in[pl.ds(t, 1)] = col_send[:, my_part][None]
     pl.semaphore_wait(barrier, lanes + groups - 2)
     over_lanes(
         0, lambda peer: col_send.at[:, pl.ds(pl.multiple_of(peer * part, part), part)], col_in.at[t]
     )
-    for p in range(lanes):
-        row_send[p] = wide[p * per_lane : (p + 1) * per_lane, :].astype(BF16)
-    row_in[pl.ds(t, 1)] = row_send[pl.ds(t, 1)]
-    over_lanes(1, lambda peer: row_send.at[peer], row_in.at[t])
 
     arrived(routes, rweight)
     chunk = pl.ds(pl.multiple_of(g // (128 // seqs) * 128, 128), 128)
@@ -195,64 +231,83 @@
     table = jnp.where((first | second) & here, 1.0, 0.0).astype(BF16)
     weighted = jnp.where(first & here, rweight[0:1], 0.0) + jnp.where(second & here, rweight[1:2], 0.0)
 
-    mine = (
-        lax.broadcasted_iota(jnp.int32, (per_lane, seqs), 1)
-        == lax.broadcasted_iota(jnp.int32, (per_lane, seqs), 0) + t * per_lane
-    ).astype(BF16)
-    hidden[...] = jnp.dot(mine, tok[...], preferred_element_type=F32)
-
     arrived(gain2)
     descriptor(0, col_in.at[pl.ds(0, lanes - 1)]).wait_recv()
-    total = tokf[:, my_part]
+    total = tok[:, my_part].astype(F32)
     for p in range(lanes):
         total = total + col_in[p].astype(F32)
     gained = (total * gain2[:, my_part]).astype(BF16)
     slots[...] = jnp.dot(table, gained, preferred_element_type=F32)
     for e in range(experts):
         disp_send[e] = slots[e * cap : (e + 1) * cap, :].astype(BF16)
-    disp_in[pl.ds(g, 1)] = disp_send[pl.ds(g, 1)]
-    over_groups(2, lambda peer: disp_send.at[peer], disp_in.at[g])
+    disp_in[pl.ds(2 * quarter + core, 1)] = disp_send[pl.ds(g, 1)]
+    to_experts()
+    slots[0:seqs, :] = total
+    for p in range(lanes):
+        row_send[p] = slots[p * per_lane : (p + 1) * per_lane, :]
+    row_in[pl.ds(t, 1)] = row_send[pl.ds(t, 1)]
+    over_lanes(1, lambda peer: row_send.at[peer], row_in.at[t])
+
+    def whole_rows(stage, side):
+        for e in range(chips * side, chips * (side + 1)):
+            slots[e * cap : (e + 1) * cap, :] = disp_in[e].astype(F32)
+        rows = slice(side * half, (side + 1) * half)
+        rows_all[rows, my_part] = slots[rows, :].astype(BF16)
+        mine = rows_all.at[pl.ds(side * half, half), my_part]
+        over_lanes(stage, lambda peer: mine, mine)
+
+    descriptor(2, disp_in.at[pl.ds(0, chips - 1)]).wait_recv()
+    whole_rows(4, 0)
 
     descriptor(1, row_in.at[pl.ds(0, lanes - 1)]).wait_recv()
+    for p in range(lanes):
+        hidden[:, p * part : (p + 1) * part] = row_in[p]
     total = hidden[...]
-    for p in range(lanes):
-        total = total + row_in[p].astype(F32)
-    hidden[...] = total
     dense_send[...] = (
         total * lax.rsqrt(jnp.mean(total * total, axis=-1, keepdims=True) + 1e-06) * gain2[...]
     ).astype(BF16)
-    dense_in[pl.ds(g, 1)] = dense_send[...][None]
-    over_groups(3, lambda peer: dense_send, dense_in.at[g])
-
-    descriptor(2, disp_in.at[pl.ds(0, groups - 1)]).wait_recv()
-    for e in range(groups):
-        slots[e * cap : (e + 1) * cap, :] = disp_in[e].astype(F32)
-    rows_all[:, my_part] = slots[...].astype(BF16)
-    over_lanes(4, lambda peer: rows_all.at[:, my_part], rows_all.at[:, my_part])
+    dense_in[pl.ds(core * chips + chip, 1)] = dense_send[...][None]
+    over_chips(9, lambda peer: dense_send, dense_in.at[core * chips + chip])
+
+    descriptor(3, disp_in.at[pl.ds(chips, chips)]).wait_recv()
+    whole_rows(5, 1)
 
     inverse = 1.0 / (gain2[...] * gain2[...])
+
+    def expert(stage, side):
+        rows = slice(side * half, (side + 1) * half)
+        squares = jnp.zeros((half, part), F32)
+        for p in range(lanes):
+            piece = rows_all[rows, p * part : (p + 1) * part].astype(F32)
+            squares = squares + piece * piece * inverse[:, p * part : (p + 1) * part]
+        scale = lax.rsqrt(jnp.sum(squares, axis=-1, keepdims=True) / width + 1e-06)
+        gate = jnp.dot(rows_all[rows, :], eg[0], preferred_element_type=F32) * scale
+        up = jnp.dot(rows_all[rows, :], eu[0], preferred_element_type=F32) * scale
+        inner = (gate * sigmoid(gate) * up).astype(BF16)
+        block = 2 * part
+        for p in range(width // block):
+            eo_send[rows, p * block : (p + 1) * block] = jnp.dot(
+                inner, ed[0, :, p * block : (p + 1) * block], preferred_element_type=F32
+            ).astype(BF16)
+        eo_in[pl.ds(t, 1), rows] = eo_send[rows, my_part][None]
+        over = pl.ds(side * half, half)
+        over_lanes(
+            stage,
+            lambda peer: eo_send.at[over, pl.ds(pl.multiple_of(peer * part, part), part)],
+            eo_in.at[t, over],
+        )
+
     arrived(eg, eu, ed)
-    descriptor(4, rows_all.at[:, pl.ds(0, width - part)]).wait_recv()
-    squares = jnp.zeros((groups * cap, part), F32)
-    for p in range(lanes):
-        piece = rows_all[:, p * part : (p + 1) * part].astype(F32)
-        squares = squares + piece * piece * inverse[:, p * part : (p + 1) * part]
-    scale = lax.rsqrt(jnp.sum(squares, axis=-1, keepdims=True) / width + 1e-06)
-    gate = jnp.dot(rows_all[...], eg[0], preferred_element_type=F32) * scale
-    up = jnp.dot(rows_all[...], eu[0], preferred_element_type=F32) * scale
-    inner = (gate * sigmoid(gate) * up).astype(BF16)
-    block = 2 * part
-    for p in range(width // block):
-        eo_send[:, p * block : (p + 1) * block] = jnp.dot(
-            inner, ed[0, :, p * block : (p + 1) * block], preferred_element_type=F32
-        ).astype(BF16)
-    eo_in[pl.ds(t, 1)] = eo_send[:, my_part][None]
-    over_lanes(
-        5, lambda peer: eo_send.at[:, pl.ds(pl.multiple_of(peer * part, part), part)], eo_in.at[t]
-    )
-
+    descriptor(4, rows_all.at[pl.ds(0, half), pl.ds(0, width - part)]).wait_recv()
+    expert(6, 0)
+    descriptor(5, rows_all.at[pl.ds(0, half), pl.ds(0, width - part)]).wait_recv()
+    expert(7, 1)
+
+    my_half, other_half = pl.ds(core * chips, chips), pl.ds((1 - core) * chips, chips)
+    descriptor(9, dense_in.at[pl.ds(0, chips - 1)]).wait_recv()
+    to_device(10, dense_in.at[my_half], dense_in.at[my_half], partner)
     arrived(dg, du, dd, goff)
-    descriptor(3, dense_in.at[pl.ds(0, groups - 1)]).wait_recv()
+    descriptor(10, dense_in.at[pl.ds(0, chips)]).wait_recv()
     for e in range(groups):
         wide[e * per_lane : (e + 1) * per_lane, :] = dense_in[e].astype(F32)
     dense_rows[...] = wide[...].astype(BF16)
@@ -264,22 +319,33 @@
     wide[...] = jnp.dot(inner, dd[...], preferred_element_type=F32)
     for e in range(groups):
         dback_send[e] = wide[e * per_lane : (e + 1) * per_lane, :].astype(BF16)
-    dback_in[pl.ds(g, 1)] = dback_send[pl.ds(g, 1)]
-
-    descriptor(5, eo_in.at[pl.ds(0, lanes - 1)]).wait_recv()
-    total = jnp.zeros((groups * cap, part), F32)
-    for p in range(lanes):
-        total = total + eo_in[p].astype(F32)
-    slots[...] = total
-    for e in range(groups):
-        back_send[e] = slots[e * cap : (e + 1) * cap, :].astype(BF16)
-    back_in[pl.ds(g, 1)] = back_send[pl.ds(g, 1)]
-    over_groups(6, lambda peer: back_send.at[peer], back_in.at[g])
-    over_groups(7, lambda peer: dback_send.at[peer], dback_in.at[g])
+    to_device(11, dback_send.at[other_half], pair_in, partner)
+
+    def expert_sums(side):
+        rows = slice(side * half, (side + 1) * half)
+        total = jnp.zeros((half, part), F32)
+        for p in range(lanes):
+            total = total + eo_in[p, rows].astype(F32)
+        slots[rows, :] = total
+        for e in range(chips * side, chips * (side + 1)):
+            back_send[e] = slots[e * cap : (e + 1) * cap, :].astype(BF16)
+
+    descriptor(6, eo_in.at[pl.ds(0, lanes - 1), pl.ds(0, half)]).wait_recv()
+    expert_sums(0)
+    back_in[pl.ds(g, 1)] = back_send[pl.ds(2 * quarter + core, 1)]
+    to_groups_near()
+    descriptor(11, pair_in).wait_recv()
+    chip_sum[...] = (dback_send[my_half].astype(F32) + pair_in[...].astype(F32)).astype(BF16)
+    dback_in[pl.ds(chip, 1)] = chip_sum[pl.ds(chip, 1)]
+    descriptor(7, eo_in.at[pl.ds(0, lanes - 1), pl.ds(0, half)]).wait_recv()
+    expert_sums(1)
+    to_groups_far()
+
+    over_chips(12, lambda peer: chip_sum.at[peer], dback_in.at[chip])
 
     upper = weighted.astype(BF16)
     lower = (weighted - upper.astype(F32)).astype(BF16)
-    descriptor(6, back_in.at[pl.ds(0, groups - 1)]).wait_recv()
+    descriptor(8, back_in.at[pl.ds(0, groups - 1)]).wait_recv()
     for e in range(experts):
         slots[e * cap : (e + 1) * cap, :] = back_in[e].astype(F32)
     back = slots[...].astype(BF16)
@@ -290,28 +356,39 @@
     for p in range(lanes):
         moe_send[p] = slots[p * per_lane : (p + 1) * per_lane, :]
     moe_in[pl.ds(t, 1)] = moe_send[pl.ds(t, 1)]
-    over_lanes(8, lambda peer: moe_send.at[peer], moe_in.at[t])
-
-    descriptor(7, dback_in.at[pl.ds(0, groups - 1)]).wait_recv()
+    over_lanes(13, lambda peer: moe_send.at[peer], moe_in.at[t])
+
+    descriptor(12, dback_in.at[pl.ds(0, chips - 1)]).wait_recv()
     total = jnp.zeros((per_lane, width), F32)
-    for e in range(groups):
+    for e in range(chips):
         total = total + dback_in[e].astype(F32)
-    base = hidden[...] + sigmoid(goff[...]) * total
-    descriptor(8, moe_in.at[pl.ds(0, lanes - 1)]).wait_recv()
+    total = hidden[...] + sigmoid(goff[...]) * total
+    descriptor(13, moe_in.at[pl.ds(0, lanes - 1)]).wait_recv()
     for p in range(lanes):
         moe_wide[:, p * part : (p + 1) * part] = moe_in[p]
-    out_ref[...] = (base + moe_wide[...]).astype(BF16)
-
-    store.wait()
-    descriptor(0, col_in.at[pl.ds(0, lanes - 1)]).wait_send()
-    descriptor(1, row_in.at[pl.ds(0, lanes - 1)]).wait_send()
-    descriptor(2, disp_in.at[pl.ds(0, groups - 1)]).wait_send()
-    descriptor(3, dense_in.at[pl.ds(0, groups - 1)]).wait_send()
-    descriptor(4, rows_all.at[:, pl.ds(0, width - part)]).wait_send()
-    descriptor(5, eo_in.at[pl.ds(0, lanes - 1)]).wait_send()
-    descriptor(6, back_in.at[pl.ds(0, groups - 1)]).wait_send()
-    descriptor(7, dback_in.at[pl.ds(0, groups - 1)]).wait_send()
-    descriptor(8, moe_in.at[pl.ds(0, lanes - 1)]).wait_send()
+    out_ref[...] = (total + moe_wide[...]).astype(BF16)
+
+    over_half = rows_all.at[pl.ds(0, half), pl.ds(0, width - part)]
+    sums_half = eo_in.at[pl.ds(0, lanes - 1), pl.ds(0, half)]
+    sent = (
+        col_in.at[pl.ds(0, lanes - 1)], row_in.at[pl.ds(0, lanes - 1)],
+        disp_in.at[pl.ds(0, chips - 1)], disp_in.at[pl.ds(0, chips)], over_half, over_half, sums_half, sums_half,
+        back_in.at[pl.ds(0, groups - 1)], dense_in.at[pl.ds(0, chips - 1)], dense_in.at[pl.ds(0, chips)], pair_in,
+        dback_in.at[pl.ds(0, chips - 1)], moe_in.at[pl.ds(0, lanes - 1)],
+    )
+    for stage, ref in enumerate(sent):
+        descriptor(stage, ref).wait_send()
+
+
+def finish_kernel(out_vmem, next_vmem, out_hbm, next_hbm, sems):
+    copies = (
+        pltpu.make_async_copy(next_vmem, next_hbm, sems.at[0]),
+        pltpu.make_async_copy(out_vmem, out_hbm, sems.at[1]),
+    )
+    for copy in copies:
+        copy.start()
+    for copy in copies:
+        copy.wait()
 
 
 def local(*args):
@@ -337,14 +414,12 @@
     held = [*held[:3], joined, *held[7:19], dense_up, *held[21:]]
     sizes = (groups, lanes, seqs, width, experts, cap)
     scratch = held + [
-        vmem((rows, 128), F32),
-        vmem((seqs, width), F32),
-        vmem((max(seqs, groups * per_lane), width), F32),
+        vmem((groups * per_lane, width), F32),
         vmem((groups * cap, part), F32),
         vmem((seqs, width), BF16),
-        vmem((lanes, per_lane, width), BF16),
+        vmem((lanes, per_lane, part), F32),
         vmem((lanes, seqs, part), BF16),
-        vmem((lanes, per_lane, width), BF16),
+        vmem((lanes, per_lane, part), F32),
         vmem((per_lane, width), F32),
         vmem((experts, cap, part), BF16),
         vmem((groups, cap, part), BF16),
@@ -353,7 +428,9 @@
         vmem((groups, per_lane, width), BF16),
         vmem((groups * per_lane, width), BF16),
         vmem((groups, per_lane, width), BF16),
-        vmem((groups, per_lane, width), BF16),
+        vmem((groups // 2, per_lane, width), BF16),
+        vmem((groups // 2, per_lane, width), BF16),
+        vmem((groups // 2, per_lane, width), BF16),
         vmem((groups * cap, width), BF16),
         vmem((lanes, groups * cap, part), BF16),
         vmem((groups, cap, part), BF16),
@@ -362,24 +439,32 @@
         vmem((lanes, per_lane, part), F32),
         vmem((per_lane, width), F32),
         pltpu.SemaphoreType.DMA((len(operands),)),
-        pltpu.SemaphoreType.DMA,
-        pltpu.SemaphoreType.DMA((9,)),
-        pltpu.SemaphoreType.DMA((9,)),
+        pltpu.SemaphoreType.DMA((14,)),
+        pltpu.SemaphoreType.DMA((14,)),
     ]
     layer_out, next_state = pl.pallas_call(
         functools.partial(layer_kernel, sizes),
-        out_shape=(
-            jax.ShapeDtypeStruct((per_lane, width), BF16),
-            jax.ShapeDtypeStruct((rows, 128), F32),
-        ),
-        in_specs=[pl.BlockSpec(memory_space=pl.ANY)] * len(operands),
-        out_specs=(pl.BlockSpec(memory_space=pltpu.VMEM), pl.BlockSpec(memory_space=pl.ANY)),
+        out_shape=(vmem((per_lane, width), BF16), vmem((rows, 128), F32)),
+        in_specs=[pl.BlockSpec(memory_space=pltpu.HBM)] * len(operands),
+        out_specs=[pl.BlockSpec(memory_space=pltpu.VMEM)] * 2,
         scratch_shapes=scratch,
         compiler_params=pltpu.CompilerParams(
             collective_id=0, has_side_effects=True, vmem_limit_bytes=60_000_000
         ),
         name="layer",
     )(*operands)
+    layer_out, next_state = pl.pallas_call(
+        finish_kernel,
+        out_shape=(
+            jax.ShapeDtypeStruct((per_lane, width), BF16),
+            jax.ShapeDtypeStruct((rows, 128), F32),
+        ),
+        in_specs=[pl.BlockSpec(memory_space=pltpu.VMEM)] * 2,
+        out_specs=[pl.BlockSpec(memory_space=pltpu.HBM)] * 2,
+        scratch_shapes=[pltpu.SemaphoreType.DMA((2,))],
+        compiler_params=pltpu.CompilerParams(vmem_limit_bytes=2_000_000),
+        name="finish",
+    )(layer_out, next_state)
     return layer_out, next_state.reshape(state.shape)
 
 

time: 73.7 us -> 57.5 us (0.78)
  Pallas kernels: 69.7 us -> 56.8 us
  local copies, waits for them, and re-layouts: 3.17 us -> 0 us
    pallas_call x1 -> x2, Pallas kernels: 69.7 us -> 56.8 us  [the longest x1 55.9 us: local(): pl.pallas_call(functools.partial(layer_kernel, sizes), out_shape=(vmem((p...]
    unnamed x2 -> x0, local copies, waits for them, and re-layouts: 3.17 us -> none
where the time goes in v2:
time: 57.5 us; the launch traced here: 57.4 us
  Pallas kernels  56.8 us (99%)
  between operations  0.65 us (1%)
    pallas_call x1, Pallas kernels, local(): pl.pallas_call(functools.partial(layer_kernel, sizes), out_shape=(vmem((p...  55.9 us

profile of v2, /device:TPU:1, one launch (start us, length us, event | category | flops | bytes accessed | tf_op | source)
XLA Modules:
  0.0 57.4 jit_solution(120409361391419314)
XLA Ops:
  0.6 55.9 %layer.1 = (bf16[2,2048]{1,0:T(2,128)(2,1)S(1)}, f32[1024,128]{1,0:T(8,128)S(1)}) custom-call(bf16[32,2048]{1,0:T(8,128)(2,1)} %refs_0_.1, f32[1024,128]{1,0:T(8,128)} %bitcast.18, f32[1,2048]{1,0:T(1,128)} %bitcast.25, bf16[64,2048]{1,0:T(8,128)(2,1)} %bitcast.21, bf16[64,2048]{1,0:T(8,128)(2,1)} %bitcast.22, bf16[64,2048]{1,0:T(8,128)(2,1)} %bitcast.23, ...), custom_call_target="tpu_custom_call" | custom-call | tf_op jit(solution)/shard_map/layer/pallas_call | solution.py:445
  56.6 0.8 %finish.1 = (bf16[2,2048]{1,0:T(2,128)(2,1)}, f32[1024,128]{1,0:T(8,128)}) custom-call(bf16[2,2048]{1,0:T(2,128)(2,1)S(1)} %get-tuple-element.6.out_vmem, f32[1024,128]{1,0:T(8,128)S(1)} %get-tuple-element.7.next_vmem), custom_call_target="tpu_custom_call" | custom-call | tf_op jit(solution)/shard_map/finish/pallas_call | solution.py:456

commit v3 on v2

--- a/solution.py
+++ b/solution.py
@@ -11,6 +11,12 @@
 MESH = pl.DeviceIdType.MESH
 F32 = jnp.float32
 BF16 = jnp.bfloat16
+ENDS = (6, 12, 16)
+PARTS = len(ENDS)
+COLUMNS, ROWS, DENSE, PASS_ON, PAIR, BLOCKS, RETURN, FINAL, DISPATCH = range(9)
+GATHER = DISPATCH + PARTS
+SUMS = GATHER + PARTS
+STAGES = SUMS + PARTS
 
 
 def sigmoid(x):
@@ -34,24 +40,13 @@
         col_send, row_send, col_in, row_in, hidden,
         disp_send, disp_in, rows_all, dense_send, dense_in, dense_rows, dback_send, dback_in, pair_in, chip_sum,
         eo_send, eo_in, back_send, back_in, moe_send, moe_in, moe_wide,
-        load_sem, send_sem, recv_sem,
+        load_sem, send_sem, recv_sem, go,
     ) = refs
     g = lax.axis_index("ep")
     t = lax.axis_index("tp")
     chips, chip, core = groups // 2, g // 2, lax.rem(g, 2)
     partner = g + 1 - 2 * core
-    quarter, half = chips // 4, groups * cap // 2
     my_part = pl.ds(pl.multiple_of(t * part, part), part)
-
-    barrier = pltpu.get_barrier_semaphore()
-
-    @pl.loop(1, lanes)
-    def _(p):
-        pl.semaphore_signal(barrier, inc=1, device_id=(g, lax.rem(t + p, lanes)), device_id_type=MESH)
-
-    @pl.loop(1, groups)
-    def _(p):
-        pl.semaphore_signal(barrier, inc=1, device_id=(lax.rem(g + p, groups), t), device_id_type=MESH)
 
     wr, wk, wv, wd = (joined.at[pl.ds(i * HEAD_WIDTH, HEAD_WIDTH)] for i in range(4))
     units = dg_hbm.shape[0]
@@ -68,21 +63,52 @@
         id(to): pltpu.make_async_copy(frm, to, load_sem.at[i])
         for i, (frm, to) in enumerate(zip(sources, targets))
     }
-    for to in targets:
+    for to in targets[:6]:
+        loads[id(to)].start()
+
+    barrier = pltpu.get_barrier_semaphore()
+
+
+    def greet(peer_group, peer_lane):
+        pl.semaphore_signal(barrier, inc=1, device_id=(peer_group, peer_lane), device_id_type=MESH)
+
+    for distance in sorted(range(1, chips), key=lambda d: -min(d, chips - d)):
+        greet(lax.rem(chip + distance, chips) * 2 + 1, t)
+    greet(partner, t)
+    for p in range(1, lanes):
+        greet(2 * chip, lax.rem(t + p, lanes))
+
+    for to in targets[6:]:
         loads[id(to)].start()
 
     def arrived(*buffers):
         for to in buffers:
             loads[id(to)].wait()
 
+    side_length = round(lanes**0.5)
+    offsets = sorted(
+        range(1, lanes),
+        key=lambda p: -sum(min(d, side_length - d) for d in divmod(p, side_length)),
+    )
+
+    def lane_at(p):
+        dy, dx = divmod(p, side_length)
+        y, x = t // side_length, lax.rem(t, side_length)
+        return lax.rem(y + dy, side_length) * side_length + lax.rem(x + dx, side_length)
+
     def over_lanes(stage, source, target):
-        @pl.loop(1, lanes)
-        def _(p):
-            peer = lax.rem(t + p, lanes)
+        for p in offsets:
+            peer = lane_at(p)
             pltpu.make_async_remote_copy(
                 src_ref=source(peer), dst_ref=target, send_sem=send_sem.at[stage],
                 recv_sem=recv_sem.at[stage], device_id=(g, peer), device_id_type=MESH,
             ).start()
+
+    apart = sorted(range(-(chips // 2), chips - chips // 2), key=lambda r: abs(r + 0.5))
+    bounds = sorted({0, *(-(-chips * end // 16) for end in ENDS)})
+    parts = len(bounds) - 1
+    places = [range(bounds[k], bounds[k + 1]) for k in range(parts)]
+    rows_of = [slice(2 * cap * bounds[k], 2 * cap * bounds[k + 1]) for k in range(parts)]
 
     def to_device(stage, source, target, peer):
         pltpu.make_async_remote_copy(
@@ -90,50 +116,31 @@
             recv_sem=recv_sem.at[stage], device_id=(peer, t), device_id_type=MESH,
         ).start()
 
+    def device_at(distance, c):
+        return lax.rem(chip + distance % chips, chips) * 2 + c
+
     def to_experts():
-        @pl.loop(chips // 2, chips)
-        def _(j):
+        for j in reversed(range(chips)):
+            stage = DISPATCH + [j in place for place in places].index(True)
+            if apart[j] == 0:
+                to_device(stage, disp_send.at[partner], disp_in.at[2 * j + core], partner)
+                continue
             for c in range(2):
-                peer = lax.rem(chip + quarter - j + chips, chips) * 2 + c
-                to_device(3, disp_send.at[peer], disp_in.at[2 * j + core], peer)
-
-        @pl.loop(1, chips // 2)
-        def _(k):
-            j = lax.rem(quarter + k, chips // 2)
+                peer = device_at(-apart[j], c)
+                to_device(stage, disp_send.at[peer], disp_in.at[2 * j + core], peer)
+
+    def to_groups(k):
+        for j in reversed(places[k]):
+            if apart[j] == 0:
+                to_device(RETURN, back_send.at[2 * j + 1 - core], back_in.at[g], partner)
+                continue
             for c in range(2):
-                peer = lax.rem(chip + quarter - j + chips, chips) * 2 + c
-                to_device(2, disp_send.at[peer], disp_in.at[2 * j + core], peer)
-
-        to_device(2, disp_send.at[partner], disp_in.at[2 * quarter + core], partner)
-
-    def to_groups_near():
-        @pl.loop(1, chips // 2)
-        def _(k):
-            j = lax.rem(quarter + k, chips // 2)
-            for c in range(2):
-                peer = lax.rem(chip + j - quarter + chips, chips) * 2 + c
-                to_device(8, back_send.at[2 * j + c], back_in.at[g], peer)
-
-        to_device(8, back_send.at[2 * quarter + 1 - core], back_in.at[g], partner)
-
-    def to_groups_far():
-        @pl.loop(chips // 2, chips)
-        def _(j):
-            for c in range(2):
-                peer = lax.rem(chip + j - quarter + chips, chips) * 2 + c
-                to_device(8, back_send.at[2 * j + c], back_in.at[g], peer)
+                to_device(RETURN, back_send.at[2 * j + c], back_in.at[g], device_at(apart[j], c))
 
     def over_chips(stage, source, target):
-        def send(distance):
+        for distance in sorted(range(1, chips), key=lambda d: -min(d, chips - d)):
             peer = lax.rem(chip + distance, chips)
             to_device(stage, source(peer), target, 2 * peer + core)
-
-        send(chips // 2)
-
-        @pl.loop(1, chips // 2)
-        def _(k):
-            send(chips // 2 - k)
-            send(chips // 2 + k)
 
     def descriptor(stage, ref):
         return pltpu.make_async_remote_copy(
@@ -202,12 +209,31 @@
     heads = heads.astype(BF16)
 
     arrived(wout)
-    col_send[...] = jnp.dot(heads, wout[...], preferred_element_type=F32).astype(BF16)
+    share = jnp.dot(heads, wout[...], preferred_element_type=F32)
+    wide[0:seqs, :] = share
+    col_send[...] = share.astype(BF16)
     col_in[pl.ds(t, 1)] = col_send[:, my_part][None]
-    pl.semaphore_wait(barrier, lanes + groups - 2)
+    @pl.when(core == 0)
+    def _():
+        pl.semaphore_wait(barrier, 2 * lanes - 1)
+        pl.semaphore_signal(go, inc=1, device_id=(partner, t), device_id_type=MESH)
+
+    @pl.when(core == 1)
+    def _():
+        pl.semaphore_wait(go, 1)
+
     over_lanes(
-        0, lambda peer: col_send.at[:, pl.ds(pl.multiple_of(peer * part, part), part)], col_in.at[t]
-    )
+        COLUMNS, lambda peer: col_send.at[:, pl.ds(pl.multiple_of(peer * part, part), part)], col_in.at[t]
+    )
+    for p in range(lanes):
+        row_send[p] = wide[p * per_lane : (p + 1) * per_lane, :].astype(BF16)
+    row_in[pl.ds(t, 1)] = row_send[pl.ds(t, 1)]
+    over_lanes(ROWS, lambda peer: row_send.at[peer], row_in.at[t])
+    mine = (
+        lax.broadcasted_iota(jnp.int32, (per_lane, seqs), 1)
+        == lax.broadcasted_iota(jnp.int32, (per_lane, seqs), 0) + t * per_lane
+    ).astype(BF16)
+    hidden[...] = jnp.dot(mine, tok[...], preferred_element_type=F32)
 
     arrived(routes, rweight)
     chunk = pl.ds(pl.multiple_of(g // (128 // seqs) * 128, 128), 128)
@@ -232,7 +258,7 @@
     weighted = jnp.where(first & here, rweight[0:1], 0.0) + jnp.where(second & here, rweight[1:2], 0.0)
 
     arrived(gain2)
-    descriptor(0, col_in.at[pl.ds(0, lanes - 1)]).wait_recv()
+    descriptor(COLUMNS, col_in.at[pl.ds(0, lanes - 1)]).wait_recv()
     total = tok[:, my_part].astype(F32)
     for p in range(lanes):
         total = total + col_in[p].astype(F32)
@@ -240,43 +266,48 @@
     slots[...] = jnp.dot(table, gained, preferred_element_type=F32)
     for e in range(experts):
         disp_send[e] = slots[e * cap : (e + 1) * cap, :].astype(BF16)
-    disp_in[pl.ds(2 * quarter + core, 1)] = disp_send[pl.ds(g, 1)]
+    disp_in[pl.ds(2 * apart.index(0) + core, 1)] = disp_send[pl.ds(g, 1)]
+
+    @pl.when(core == 1)
+    def _():
+        pl.semaphore_wait(barrier, 2 * chips - 1)
+        pl.semaphore_signal(go, inc=1, device_id=(partner, t), device_id_type=MESH)
+
+    @pl.when(core == 0)
+    def _():
+        pl.semaphore_wait(go, 1)
+
     to_experts()
-    slots[0:seqs, :] = total
+
+    descriptor(ROWS, row_in.at[pl.ds(0, lanes - 1)]).wait_recv()
+    total = hidden[...]
     for p in range(lanes):
-        row_send[p] = slots[p * per_lane : (p + 1) * per_lane, :]
-    row_in[pl.ds(t, 1)] = row_send[pl.ds(t, 1)]
-    over_lanes(1, lambda peer: row_send.at[peer], row_in.at[t])
-
-    def whole_rows(stage, side):
-        for e in range(chips * side, chips * (side + 1)):
-            slots[e * cap : (e + 1) * cap, :] = disp_in[e].astype(F32)
-        rows = slice(side * half, (side + 1) * half)
-        rows_all[rows, my_part] = slots[rows, :].astype(BF16)
-        mine = rows_all.at[pl.ds(side * half, half), my_part]
-        over_lanes(stage, lambda peer: mine, mine)
-
-    descriptor(2, disp_in.at[pl.ds(0, chips - 1)]).wait_recv()
-    whole_rows(4, 0)
-
-    descriptor(1, row_in.at[pl.ds(0, lanes - 1)]).wait_recv()
-    for p in range(lanes):
-        hidden[:, p * part : (p + 1) * part] = row_in[p]
-    total = hidden[...]
+        total = total + row_in[p].astype(F32)
+    hidden[...] = total
     dense_send[...] = (
         total * lax.rsqrt(jnp.mean(total * total, axis=-1, keepdims=True) + 1e-06) * gain2[...]
     ).astype(BF16)
     dense_in[pl.ds(core * chips + chip, 1)] = dense_send[...][None]
-    over_chips(9, lambda peer: dense_send, dense_in.at[core * chips + chip])
-
-    descriptor(3, disp_in.at[pl.ds(chips, chips)]).wait_recv()
-    whole_rows(5, 1)
+    over_chips(DENSE, lambda peer: dense_send, dense_in.at[core * chips + chip])
+
+    def whole_rows(k):
+        rows = rows_of[k]
+        for e in range(rows.start // cap, rows.stop // cap):
+            slots[e * cap : (e + 1) * cap, :] = disp_in[e].astype(F32)
+        rows_all[rows, my_part] = slots[rows, :].astype(BF16)
+        mine = rows_all.at[rows, my_part]
+        over_lanes(GATHER + k, lambda peer: mine, mine)
+
+    packets = [2 * len(places[k]) - (k == 0) for k in range(parts)]
+    for k in range(parts):
+        descriptor(DISPATCH + k, disp_in.at[pl.ds(0, packets[k])]).wait_recv()
+        whole_rows(k)
 
     inverse = 1.0 / (gain2[...] * gain2[...])
 
-    def expert(stage, side):
-        rows = slice(side * half, (side + 1) * half)
-        squares = jnp.zeros((half, part), F32)
+    def expert(k):
+        rows = rows_of[k]
+        squares = jnp.zeros((rows.stop - rows.start, part), F32)
         for p in range(lanes):
             piece = rows_all[rows, p * part : (p + 1) * part].astype(F32)
             squares = squares + piece * piece * inverse[:, p * part : (p + 1) * part]
@@ -290,24 +321,23 @@
                 inner, ed[0, :, p * block : (p + 1) * block], preferred_element_type=F32
             ).astype(BF16)
         eo_in[pl.ds(t, 1), rows] = eo_send[rows, my_part][None]
-        over = pl.ds(side * half, half)
         over_lanes(
-            stage,
-            lambda peer: eo_send.at[over, pl.ds(pl.multiple_of(peer * part, part), part)],
-            eo_in.at[t, over],
+            SUMS + k,
+            lambda peer: eo_send.at[rows, pl.ds(pl.multiple_of(peer * part, part), part)],
+            eo_in.at[t, rows],
         )
 
+    my_half, other_half = pl.ds(core * chips, chips), pl.ds((1 - core) * chips, chips)
+    descriptor(DENSE, dense_in.at[pl.ds(0, chips - 1)]).wait_recv()
+    to_device(PASS_ON, dense_in.at[my_half], dense_in.at[my_half], partner)
+
+    gathered = [rows_all.at[rows, pl.ds(0, width - part)] for rows in rows_of]
     arrived(eg, eu, ed)
-    descriptor(4, rows_all.at[pl.ds(0, half), pl.ds(0, width - part)]).wait_recv()
-    expert(6, 0)
-    descriptor(5, rows_all.at[pl.ds(0, half), pl.ds(0, width - part)]).wait_recv()
-    expert(7, 1)
-
-    my_half, other_half = pl.ds(core * chips, chips), pl.ds((1 - core) * chips, chips)
-    descriptor(9, dense_in.at[pl.ds(0, chips - 1)]).wait_recv()
-    to_device(10, dense_in.at[my_half], dense_in.at[my_half], partner)
+    descriptor(GATHER, gathered[0]).wait_recv()
+    expert(0)
+
     arrived(dg, du, dd, goff)
-    descriptor(10, dense_in.at[pl.ds(0, chips)]).wait_recv()
+    descriptor(PASS_ON, dense_in.at[pl.ds(0, chips)]).wait_recv()
     for e in range(groups):
         wide[e * per_lane : (e + 1) * per_lane, :] = dense_in[e].astype(F32)
     dense_rows[...] = wide[...].astype(BF16)
@@ -319,33 +349,40 @@
     wide[...] = jnp.dot(inner, dd[...], preferred_element_type=F32)
     for e in range(groups):
         dback_send[e] = wide[e * per_lane : (e + 1) * per_lane, :].astype(BF16)
-    to_device(11, dback_send.at[other_half], pair_in, partner)
-
-    def expert_sums(side):
-        rows = slice(side * half, (side + 1) * half)
-        total = jnp.zeros((half, part), F32)
+    to_device(PAIR, dback_send.at[other_half], pair_in, partner)
+
+    def dense_sums_out():
+        descriptor(PAIR, pair_in).wait_recv()
+        chip_sum[...] = (dback_send[my_half].astype(F32) + pair_in[...].astype(F32)).astype(BF16)
+        dback_in[pl.ds(chip, 1)] = chip_sum[pl.ds(chip, 1)]
+        over_chips(BLOCKS, lambda peer: chip_sum.at[peer], dback_in.at[chip])
+
+    for k in range(1, parts):
+        descriptor(GATHER + k, gathered[k]).wait_recv()
+        expert(k)
+        if k == 1:
+            dense_sums_out()
+
+    def expert_sums(k):
+        rows = rows_of[k]
+        total = jnp.zeros((rows.stop - rows.start, part), F32)
         for p in range(lanes):
             total = total + eo_in[p, rows].astype(F32)
         slots[rows, :] = total
-        for e in range(chips * side, chips * (side + 1)):
+        for e in range(rows.start // cap, rows.stop // cap):
             back_send[e] = slots[e * cap : (e + 1) * cap, :].astype(BF16)
 
-    descriptor(6, eo_in.at[pl.ds(0, lanes - 1), pl.ds(0, half)]).wait_recv()
-    expert_sums(0)
-    back_in[pl.ds(g, 1)] = back_send[pl.ds(2 * quarter + core, 1)]
-    to_groups_near()
-    descriptor(11, pair_in).wait_recv()
-    chip_sum[...] = (dback_send[my_half].astype(F32) + pair_in[...].astype(F32)).astype(BF16)
-    dback_in[pl.ds(chip, 1)] = chip_sum[pl.ds(chip, 1)]
-    descriptor(7, eo_in.at[pl.ds(0, lanes - 1), pl.ds(0, half)]).wait_recv()
-    expert_sums(1)
-    to_groups_far()
-
-    over_chips(12, lambda peer: chip_sum.at[peer], dback_in.at[chip])
+    summed = [eo_in.at[pl.ds(0, lanes - 1), rows] for rows in rows_of]
+    for k in range(parts):
+        descriptor(SUMS + k, summed[k]).wait_recv()
+        expert_sums(k)
+        if k == 0:
+            back_in[pl.ds(g, 1)] = back_send[pl.ds(2 * apart.index(0) + core, 1)]
+        to_groups(k)
 
     upper = weighted.astype(BF16)
     lower = (weighted - upper.astype(F32)).astype(BF16)
-    descriptor(8, back_in.at[pl.ds(0, groups - 1)]).wait_recv()
+    descriptor(RETURN, back_in.at[pl.ds(0, groups - 1)]).wait_recv()
     for e in range(experts):
         slots[e * cap : (e + 1) * cap, :] = back_in[e].astype(F32)
     back = slots[...].astype(BF16)
@@ -356,27 +393,31 @@
     for p in range(lanes):
         moe_send[p] = slots[p * per_lane : (p + 1) * per_lane, :]
     moe_in[pl.ds(t, 1)] = moe_send[pl.ds(t, 1)]
-    over_lanes(13, lambda peer: moe_send.at[peer], moe_in.at[t])
-
-    descriptor(12, dback_in.at[pl.ds(0, chips - 1)]).wait_recv()
+    over_lanes(FINAL, lambda peer: moe_send.at[peer], moe_in.at[t])
+
+    descriptor(BLOCKS, dback_in.at[pl.ds(0, chips - 1)]).wait_recv()
     total = jnp.zeros((per_lane, width), F32)
     for e in range(chips):
         total = total + dback_in[e].astype(F32)
     total = hidden[...] + sigmoid(goff[...]) * total
-    descriptor(13, moe_in.at[pl.ds(0, lanes - 1)]).wait_recv()
+    descriptor(FINAL, moe_in.at[pl.ds(0, lanes - 1)]).wait_recv()
     for p in range(lanes):
         moe_wide[:, p * part : (p + 1) * part] = moe_in[p]
     out_ref[...] = (total + moe_wide[...]).astype(BF16)
 
-    over_half = rows_all.at[pl.ds(0, half), pl.ds(0, width - part)]
-    sums_half = eo_in.at[pl.ds(0, lanes - 1), pl.ds(0, half)]
-    sent = (
-        col_in.at[pl.ds(0, lanes - 1)], row_in.at[pl.ds(0, lanes - 1)],
-        disp_in.at[pl.ds(0, chips - 1)], disp_in.at[pl.ds(0, chips)], over_half, over_half, sums_half, sums_half,
-        back_in.at[pl.ds(0, groups - 1)], dense_in.at[pl.ds(0, chips - 1)], dense_in.at[pl.ds(0, chips)], pair_in,
-        dback_in.at[pl.ds(0, chips - 1)], moe_in.at[pl.ds(0, lanes - 1)],
-    )
-    for stage, ref in enumerate(sent):
+    sent = {
+        COLUMNS: col_in.at[pl.ds(0, lanes - 1)],
+        ROWS: row_in.at[pl.ds(0, lanes - 1)],
+        DENSE: dense_in.at[pl.ds(0, chips - 1)],
+        PASS_ON: dense_in.at[pl.ds(0, chips)],
+        PAIR: pair_in,
+        BLOCKS: dback_in.at[pl.ds(0, chips - 1)],
+        RETURN: back_in.at[pl.ds(0, groups - 1)],
+        FINAL: moe_in.at[pl.ds(0, lanes - 1)],
+    }
+    for k in range(parts):
+        sent |= {DISPATCH + k: disp_in.at[pl.ds(0, packets[k])], GATHER + k: gathered[k], SUMS + k: summed[k]}
+    for stage, ref in sent.items():
         descriptor(stage, ref).wait_send()
 
 
@@ -417,9 +458,9 @@
         vmem((groups * per_lane, width), F32),
         vmem((groups * cap, part), F32),
         vmem((seqs, width), BF16),
-        vmem((lanes, per_lane, part), F32),
+        vmem((lanes, per_lane, width), BF16),
         vmem((lanes, seqs, part), BF16),
-        vmem((lanes, per_lane, part), F32),
+        vmem((lanes, per_lane, width), BF16),
         vmem((per_lane, width), F32),
         vmem((experts, cap, part), BF16),
         vmem((groups, cap, part), BF16),
@@ -439,8 +480,9 @@
         vmem((lanes, per_lane, part), F32),
         vmem((per_lane, width), F32),
         pltpu.SemaphoreType.DMA((len(operands),)),
-        pltpu.SemaphoreType.DMA((14,)),
-        pltpu.SemaphoreType.DMA((14,)),
+        pltpu.SemaphoreType.DMA((STAGES,)),
+        pltpu.SemaphoreType.DMA((STAGES,)),
+        pltpu.SemaphoreType.REGULAR,
     ]
     layer_out, next_state = pl.pallas_call(
         functools.partial(layer_kernel, sizes),

time: 57.5 us -> 55.8 us (0.970)
  Pallas kernels: 56.8 us -> 55 us
    pallas_call x1, Pallas kernels: 55.9 us -> 54.2 us  [local(): pl.pallas_call(functools.partial(layer_kernel, sizes), out_shape=(vmem((p...]
where the time goes in v3:
time: 55.8 us; the launch traced here: 55.7 us
  Pallas kernels  55 us (99%)
  between operations  0.65 us (1%)
    pallas_call x1, Pallas kernels, local(): pl.pallas_call(functools.partial(layer_kernel, sizes), out_shape=(vmem((p...  54.2 us

profile of v3, /device:TPU:1, one launch (start us, length us, event | category | flops | bytes accessed | tf_op | source)
XLA Modules:
  0.0 55.7 jit_solution(1345010658192462393)
XLA Ops:
  0.6 54.2 %layer.1 = (bf16[2,2048]{1,0:T(2,128)(2,1)S(1)}, f32[1024,128]{1,0:T(8,128)S(1)}) custom-call(bf16[32,2048]{1,0:T(8,128)(2,1)} %refs_0_.1, f32[1024,128]{1,0:T(8,128)} %bitcast.18, f32[1,2048]{1,0:T(1,128)} %bitcast.25, bf16[64,2048]{1,0:T(8,128)(2,1)} %bitcast.21, bf16[64,2048]{1,0:T(8,128)(2,1)} %bitcast.22, bf16[64,2048]{1,0:T(8,128)(2,1)} %bitcast.23, ...), custom_call_target="tpu_custom_call" | custom-call | tf_op jit(solution)/shard_map/layer/pallas_call | solution.py:487
  54.9 0.8 %finish.1 = (bf16[2,2048]{1,0:T(2,128)(2,1)}, f32[1024,128]{1,0:T(8,128)}) custom-call(bf16[2,2048]{1,0:T(2,128)(2,1)S(1)} %get-tuple-element.6.out_vmem, f32[1024,128]{1,0:T(8,128)S(1)} %get-tuple-element.7.next_vmem), custom_call_target="tpu_custom_call" | custom-call | tf_op jit(solution)/shard_map/finish/pallas_call | solution.py:498
